TPU v7x, 128 devices: a whole 4x4x4 slice. The times are simulated.
128 devices in a mesh: fs: 16 (over z, x), tp: 8 (over y, core).
Axes of the slice: x: 4, y: 4, z: 4, core: 2. Of those that a mesh axis runs over, the one named last changes fastest.
Arguments:
- stream: bfloat16 [8192, 2048], P('fs', 'tp'), may hold values from -6 to 6
- gain_mix: float32 [2048], replicated, may hold values from 0.1 to 1.9
- pool_weight: bfloat16 [4, 512, 512], P(None, 'fs', 'tp'), may hold values from -0.25 to 0.25
- pool_gain: float32 [2048], replicated, may hold values from 0.1 to 1.9
- gain_ffn: float32 [2048], replicated, may hold values from 0.1 to 1.9
- gate_weight: bfloat16 [2048, 5632], P('fs', 'tp'), may hold values from -0.125 to 0.125
- up_weight: bfloat16 [2048, 5632], P('fs', 'tp'), may hold values from -0.125 to 0.125
- gate_taps: float32 [3, 5632], replicated, may hold values from -2.5 to 2.5
- up_taps: float32 [3, 5632], replicated, may hold values from -2.5 to 2.5
- down_weight: bfloat16 [5632, 2048], P('tp', 'fs'), may hold values from -0.078125 to 0.078125
Outputs:
- layer_out: bfloat16 [8192, 2048], P('fs', 'tp')
All inputs are finite; a program needn't handle non-finite values.
Results may differ from a plain program's by a relative error of at most 0.01.
Values may be sent and summed in bfloat16 or wider, within the bound.
A program may use at most 64 MiB of HBM per device.

v0:
```python
import jax
import jax.numpy as jnp
from jax import lax
from jax.sharding import PartitionSpec as P

LEN = 128


epsilon = 1e-06


def in_order(tiles, dim):
    tiles = jnp.moveaxis(tiles, 0, dim)
    lengths = tiles.shape
    return tiles.reshape(*lengths[:dim], lengths[dim] * lengths[dim + 1], *lengths[dim + 2 :])


def from_everyone(shard, axis):
    copies = jnp.broadcast_to(shard, (lax.axis_size(axis), *shard.shape))
    return lax.all_to_all(copies, axis, split_axis=0, concat_axis=0, tiled=True)


def gathered_copies(shard, axis, dim):
    return in_order(from_everyone(shard, axis), dim)


def sent_together(arrays, axis, dim, along):
    both = jnp.concatenate(arrays, axis=along)
    out, at, outs = (lax.all_gather(both, axis, axis=dim, tiled=True), 0, [])
    for a in arrays:
        outs.append(lax.slice_in_dim(out, at, at + a.shape[along], axis=along))
        at += a.shape[along]
    return tuple(outs)


def rms_norm(values, scales):
    return values * lax.rsqrt(jnp.mean(values * values, axis=-1, keepdims=True) + epsilon) * scales


def delayed(values, amount):
    return jnp.pad(values, ((0, 0), (amount, 0), (0, 0)))[:, : values.shape[1]]


def pool_less(values):
    channels = values.shape[2]
    group_id = jnp.arange(channels) % 4
    partials = [values]
    running = values
    for amount in (1, 2, 4, 8):
        running = running + delayed(running, amount)
        partials.append(running)
    picked = jnp.where(
        group_id == 0,
        partials[1],
        jnp.where(group_id == 1, partials[2], jnp.where(group_id == 2, partials[3], partials[4])),
    )
    extent = jnp.where(
        group_id == 0, 2.0, jnp.where(group_id == 1, 4.0, jnp.where(group_id == 2, 8.0, 16.0))
    )
    position = jnp.arange(values.shape[1]).astype(jnp.float32)[:, None] + 1.0
    divisor = jnp.minimum(position, extent[None, :])
    return picked / divisor[None] - values


def causal_taps(values, kernel):
    reach = kernel.shape[0]
    length = values.shape[1]
    padded = jnp.pad(values, ((0, 0), (reach - 1, 0), (0, 0)))
    running = padded[:, 0:length] * kernel[0]
    for shift_by in range(1, reach):
        running = running + padded[:, shift_by : shift_by + length] * kernel[shift_by]
    return running


def add_rows(left, portion):
    return jnp.dot(left, portion, preferred_element_type=jnp.float32)


def body(
    stream,
    gain_mix,
    pool_weight,
    pool_gain,
    gain_ffn,
    gate_weight,
    up_weight,
    gate_taps,
    up_taps,
    down_weight,
):
    tok_rows, own_cols = stream.shape
    seq_count = tok_rows // LEN
    gathered = gathered_copies(stream, "tp", 1)
    channels = gathered.shape[1]
    normed = lax.optimization_barrier(
        rms_norm(gathered.astype(jnp.float32), gain_mix).astype(jnp.bfloat16)
    )
    pooled = pool_less(normed.astype(jnp.float32).reshape(seq_count, LEN, channels)).astype(
        jnp.bfloat16
    )
    pooled = pooled.reshape(tok_rows, channels // 4, 4)
    pool_part = gathered_copies(pool_weight, "fs", 1)
    pool_full = gathered_copies(pool_part, "tp", 2)
    mixer = (
        jnp.einsum("tcg,gce->teg", pooled, pool_full, preferred_element_type=jnp.float32).reshape(
            tok_rows, channels
        )
        * pool_gain
    )
    middle = lax.optimization_barrier((gathered.astype(jnp.float32) + mixer).astype(jnp.bfloat16))
    normed_ffn = rms_norm(middle.astype(jnp.float32), gain_ffn).astype(jnp.bfloat16)
    hidden_cols = gate_weight.shape[1]
    portions = sent_together((gate_weight, up_weight), "fs", 0, 1)
    gate_sum = add_rows(normed_ffn, portions[0])
    value_sum = add_rows(normed_ffn, portions[1])
    gate_proj = lax.optimization_barrier(gate_sum.astype(jnp.bfloat16))
    value_proj = lax.optimization_barrier(value_sum.astype(jnp.bfloat16))
    column_start = lax.axis_index("tp") * hidden_cols
    gate_kernel = lax.dynamic_slice_in_dim(gate_taps, column_start, hidden_cols, 1)
    value_kernel = lax.dynamic_slice_in_dim(up_taps, column_start, hidden_cols, 1)
    gate_conv = causal_taps(
        gate_proj.astype(jnp.float32).reshape(seq_count, LEN, hidden_cols), gate_kernel
    )
    value_conv = causal_taps(
        value_proj.astype(jnp.float32).reshape(seq_count, LEN, hidden_cols), value_kernel
    )
    hidden = (
        (jax.nn.silu(gate_conv) * value_conv).astype(jnp.bfloat16).reshape(tok_rows, hidden_cols)
    )
    partial_value = jnp.dot(
        hidden, gathered_copies(down_weight, "fs", 1), preferred_element_type=jnp.float32
    )
    return lax.psum_scatter(partial_value, "tp", scatter_dimension=1, tiled=True).astype(
        jnp.bfloat16
    )


def solution(mesh):
    return jax.shard_map(
        body,
        mesh=mesh,
        in_specs=(
            P("fs", "tp"),
            P(),
            P(None, "fs", "tp"),
            P(),
            P(),
            P("fs", "tp"),
            P("fs", "tp"),
            P(),
            P(),
            P("tp", "fs"),
        ),
        out_specs=P("fs", "tp"),
        check_vma=False,
    )
```

profile of v0, /device:TPU:0, one launch (start us, length us, event | category | flops | bytes accessed | tf_op | source)
XLA Modules:
  0.0 208.6 jit_solution(15406191172936369108)
XLA Ops:
  6.5 1.8 pad_maximum_fusion
  10.3 8.0 %all-to-all-start.1 = ((bf16[16,2,4096]{2,1,0:T(2,128)(2,1)}), bf16[16,2,4096]{2,1,0:T(2,128)(2,1)S(1)}, u32[]{:S(2)}, u32[]{:S(2)}) async-start(bf16[16,2,4096]{2,1,0:T(2,128)(2,1)} %reshape.137), calls=%async_computation.1 | async-start | bytes 524288 | tf_op jit(solution)/shard_map/all_to_all | solution.py:20
  18.5 8.5 %all-to-all-done.1 = bf16[16,2,4096]{2,1,0:T(2,128)(2,1)S(1)} async-done(((bf16[16,2,4096]{2,1,0:T(2,128)(2,1)}), bf16[16,2,4096]{2,1,0:T(2,128)(2,1)S(1)}, u32[]{:S(2)}, u32[]{:S(2)}) %all-to-all-start.1) | async-done | bytes 262176 | tf_op jit(solution)/shard_map/all_to_all | solution.py:20
  27.0 1.5 broadcast_in_dim.45
  28.5 4.5 %all-to-all-start = ((bf16[8,512,256]{1,2,0:T(8,128)(2,1)}), bf16[8,512,256]{1,2,0:T(8,128)(2,1)S(1)}, u32[]{:S(2)}, u32[]{:S(2)}) async-start(bf16[8,512,256]{1,2,0:T(8,128)(2,1)} %broadcast_in_dim.45), calls=%async_computation | async-start | bytes 4194304 | tf_op jit(solution)/shard_map/all_to_all | solution.py:20
  33.0 1.5 dynamic-slice_reduce_fusion.2
  36.1 1.9 copy.17
  39.3 20.9 %all-to-all-done = bf16[8,512,256]{1,2,0:T(8,128)(2,1)S(1)} async-done(((bf16[8,512,256]{1,2,0:T(8,128)(2,1)}), bf16[8,512,256]{1,2,0:T(8,128)(2,1)S(1)}, u32[]{:S(2)}, u32[]{:S(2)}) %all-to-all-start) | async-done | bytes 2097184 | tf_op jit(solution)/shard_map/all_to_all | solution.py:20
  60.2 1.6 broadcast_in_dim.54
  61.8 4.5 %all-to-all-start.2 = ((bf16[8,4,512,64]{2,3,1,0:T(8,128)(2,1)}), bf16[8,4,512,64]{2,3,1,0:T(8,128)(2,1)}, u32[]{:S(2)}, u32[]{:S(2)}) async-start(bf16[8,4,512,64]{2,3,1,0:T(8,128)(2,1)} %broadcast_in_dim.54), calls=%async_computation.2 | async-start | bytes 4194304 | tf_op jit(solution)/shard_map/all_to_all | solution.py:20
  66.8 1.9 fusion.10
  68.7 4.8 %reshape.126 = f32[4,128,2048]{1,0,2:T(4,128)} reshape(bf16[512,2048]{0,1:T(8,128)(2,1)} %fusion.10) | data formatting | bytes 6291456 | tf_op jit(solution)/shard_map/reshape | solution.py:98
  73.6 5.5 %fusion.5 = f32[4,128,2048]{1,0,2:T(4,128)S(1)} fusion(f32[4,128,2048]{1,0,2:T(4,128)} %reshape.126), kind=kLoop, calls=%fused_computation.13 | loop fusion | flops 1048576 | bytes 8388608 | tf_op jit(solution)/shard_map/add | solution.py:50
  79.1 2.3 %fusion.6 = f32[4,128,2048]{1,0,2:T(4,128)S(1)} fusion(f32[4,128,2048]{1,0,2:T(4,128)S(1)} %fusion.5), kind=kLoop, calls=%fused_computation.14 | loop fusion | flops 1048576 | bytes 8388608 | tf_op jit(solution)/shard_map/add | solution.py:50
  81.4 2.3 %fusion.7 = f32[4,128,2048]{1,0,2:T(4,128)S(1)} fusion(f32[4,128,2048]{1,0,2:T(4,128)S(1)} %fusion.6), kind=kLoop, calls=%fused_computation.15 | loop fusion | flops 1048576 | bytes 8388608 | tf_op jit(solution)/shard_map/add | solution.py:50
  83.8 16.9 %fusion.12 = bf16[4,128,2048]{1,0,2:T(4,128)(2,1)} fusion(f32[4,128,2048]{1,0,2:T(4,128)S(1)} %copy-done, f32[4,128,2048]{1,0,2:T(4,128)S(1)} %fusion.5, f32[4,128,2048]{1,0,2:T(4,128)S(1)} %fusion.7, f32[128,2048]{0,1:T(8,128)S(1)} %broadcast_minimum_fusion, pred[2048]{0:T(1024)(128)(4,1)S(1)} %get-tuple-element.11, ...), kind=kLoop, calls=%fused_computation.23 | loop fusion | flops 8388608 | bytes 15734784 | tf_op jit(solution)/shard_map/convert_element_type | solution.py:98
  100.7 4.1 %reshape.114 = bf16[512,512,4]{0,2,1:T(4,128)(2,1)} reshape(bf16[4,128,2048]{1,0,2:T(4,128)(2,1)} %fusion.12) | data formatting | bytes 4194304 | tf_op jit(solution)/shard_map/reshape | solution.py:101
  104.9 2.1 %broadcast_in_dim.55 = bf16[16,704,128]{2,1,0:T(8,128)(2,1)} broadcast(bf16[704,128]{1,0:T(8,128)(2,1)S(1)} %copy-done.5), dimensions={1,2} | broadcast | bytes 3063808 | tf_op jit(solution)/shard_map/broadcast_in_dim | solution.py:19
  107.0 4.5 %all-to-all-start.3 = ((bf16[16,704,128]{2,1,0:T(8,128)(2,1)}), bf16[16,704,128]{2,1,0:T(8,128)(2,1)}, u32[]{:S(2)}, u32[]{:S(2)}) async-start(bf16[16,704,128]{2,1,0:T(8,128)(2,1)} %broadcast_in_dim.55), calls=%async_computation.3 | async-start | bytes 5767168 | tf_op jit(solution)/shard_map/all_to_all | solution.py:20
  111.8 1.9 copy.19
  115.3 4.7 %copy.21 = f32[512,512,4]{0,2,1:T(4,128)} copy(f32[512,512,4]{0,1,2:T(8,128)S(1)} %convolution_bitcast_fusion) | data formatting | bytes 8388608 | tf_op jit(solution)/shard_map/tcg,gce->teg/transpose | solution.py:105
  120.1 5.3 %reshape.117 = f32[512,2048]{0,1:T(8,128)} reshape(f32[512,512,4]{0,2,1:T(4,128)} %copy.21) | data formatting | bytes 8388608 | tf_op jit(solution)/shard_map/reshape | solution.py:105
  125.4 2.7 %fusion.11 = bf16[512,2048]{0,1:T(8,128)(2,1)S(1)} fusion(bf16[8,512,256]{1,2,0:T(8,128)(2,1)S(1)} %all-to-all-done, f32[512,2048]{0,1:T(8,128)} %reshape.117, f32[2048]{0:T(1024)S(1)} %copy-done.7), kind=kLoop, calls=%fused_computation.22 | loop fusion | flops 4194304 | bytes 8396800 | tf_op jit(solution)/shard_map/convert_element_type | solution.py:110
  130.6 5.1 %fusion.31 = bf16[512,704]{0,1:T(8,128)(2,1)} fusion(bf16[2048,1408]{0,1:T(8,128)(2,1)} %all-gather.2.cloned.1.call-done, bf16[512,2048]{0,1:T(8,128)(2,1)} %copy-done.2, f32[2048]{0:T(1024)S(1)} %copy-done.9, f32[512]{0:T(512)S(1)} %add_rsqrt_fusion), kind=kOutput, calls=%fused_computation.48 | convolution fusion | flops 1480949760 | bytes 5711872 | tf_op jit(solution)/shard_map/dot_general | solution.py:76
  135.7 1.7 reshape.128
  137.4 4.4 %fusion.34 = bf16[512,704]{0,1:T(8,128)(2,1)} fusion(bf16[2048,1408]{0,1:T(8,128)(2,1)} %all-gather.2.cloned.1.call-done, bf16[512,2048]{0,1:T(8,128)(2,1)S(1)} %copy-done.3, f32[2048]{0:T(1024)} %param.14, f32[512]{0:T(512)} %copy-done.8), kind=kOutput, calls=%fused_computation.49 | convolution fusion | flops 1480949760 | bytes 5711872 | tf_op jit(solution)/shard_map/dot_general | solution.py:76
  141.9 1.7 reshape.130
  143.6 10.6 %fusion.30 = bf16[4,128,704]{1,0,2:T(4,128)(2,1)} fusion(f32[4,128,704]{1,0,2:T(4,128)S(1)} %reshape.130, f32[4,128,704]{1,0,2:T(4,128)S(1)} %reshape.128, f32[704]{0:T(1024)S(1)} %get-tuple-element.10, f32[704]{0:T(1024)S(1)} %get-tuple-element.9, f32[704]{0:T(1024)S(1)} %get-tuple-element.8, f32[704]{0:T(1024)S(1)} %get-tuple-element.13, ...), kind=kLoop, calls=%fused_computation.47 | loop fusion | flops 5767168 | bytes 3621376 | tf_op jit(solution)/shard_map/convert_element_type | solution.py:128
  154.2 3.2 %all-to-all-done.3 = bf16[16,704,128]{2,1,0:T(8,128)(2,1)} async-done(((bf16[16,704,128]{2,1,0:T(8,128)(2,1)}), bf16[16,704,128]{2,1,0:T(8,128)(2,1)}, u32[]{:S(2)}, u32[]{:S(2)}) %all-to-all-start.3) | async-done | bytes 2883616 | tf_op jit(solution)/shard_map/all_to_all | solution.py:20
  157.3 5.8 %fusion.13 = f32[512,2048]{1,0:T(8,128)} fusion(bf16[88,8,4,128]{3,2,1,0:T(4,128)(2,1)} %bitcast.45, bf16[16,704,128]{2,1,0:T(8,128)(2,1)} %all-to-all-done.3), kind=kOutput, calls=%fused_computation.28 | convolution fusion | flops 1476395008 | bytes 7798784 | tf_op jit(solution)/shard_map/dot_general | solution.py:130
  163.2 36.8 %reduce-scatter.2.cloned.1.call-done = f32[512,256]{1,0:T(8,128)} async-done(((f32[512,2048]{1,0:T(8,128)}), f32[512,256]{1,0:T(8,128)}) %reduce-scatter.2.cloned.1.call-update) | async-done | bytes 524304 | tf_op jit(solution)/shard_map/reduce_scatter | solution.py:133
  200.0 1.8 convert_element_type.75
  (41 shorter events, 9.8 us)
Async XLA Ops:
  6.5 11.8 %copy-start.4 = (bf16[512,256]{1,0:T(8,128)(2,1)S(1)}, bf16[512,256]{1,0:T(8,128)(2,1)}, u32[]{:S(2)}) copy-start(bf16[512,256]{1,0:T(8,128)(2,1)} %param.10) | copy-start | bytes 786436
  6.5 123.5 %all-gather.2.cloned.1.call-start = ((), (), s32[]{:S(2)}) async-start(), calls=%async_computation.5 | async-start | bytes 6127616 | tf_op jit(solution)/shard_map/all_gather | solution.py:29
  10.3 16.7 %all-to-all-start.1 = ((bf16[16,2,4096]{2,1,0:T(2,128)(2,1)}), bf16[16,2,4096]{2,1,0:T(2,128)(2,1)S(1)}, u32[]{:S(2)}, u32[]{:S(2)}) async-start(bf16[16,2,4096]{2,1,0:T(2,128)(2,1)} %reshape.137), calls=%async_computation.1 | async-start | bytes 524288 | tf_op jit(solution)/shard_map/all_to_all | solution.py:20
  28.5 31.6 %all-to-all-start = ((bf16[8,512,256]{1,2,0:T(8,128)(2,1)}), bf16[8,512,256]{1,2,0:T(8,128)(2,1)S(1)}, u32[]{:S(2)}, u32[]{:S(2)}) async-start(bf16[8,512,256]{1,2,0:T(8,128)(2,1)} %broadcast_in_dim.45), calls=%async_computation | async-start | bytes 4194304 | tf_op jit(solution)/shard_map/all_to_all | solution.py:20
  61.8 5.0 %copy-start.6 = (f32[2048]{0:T(1024)S(1)}, f32[2048]{0:T(1024)}, u32[]{:S(2)}) copy-start(f32[2048]{0:T(1024)} %param.11) | copy-start | bytes 24580
  61.8 43.1 %all-to-all-start.2 = ((bf16[8,4,512,64]{2,3,1,0:T(8,128)(2,1)}), bf16[8,4,512,64]{2,3,1,0:T(8,128)(2,1)}, u32[]{:S(2)}, u32[]{:S(2)}) async-start(bf16[8,4,512,64]{2,3,1,0:T(8,128)(2,1)} %broadcast_in_dim.54), calls=%async_computation.2 | async-start | bytes 4194304 | tf_op jit(solution)/shard_map/all_to_all | solution.py:20
  81.4 2.3 %copy-start = (f32[4,128,2048]{1,0,2:T(4,128)S(1)}, f32[4,128,2048]{1,0,2:T(4,128)}, u32[]{:S(2)}) copy-start(f32[4,128,2048]{1,0,2:T(4,128)} %reshape.126) | copy-start | bytes 12582916
  100.7 4.2 %copy-start.5 = (bf16[704,128]{1,0:T(8,128)(2,1)S(1)}, bf16[704,128]{1,0:T(8,128)(2,1)}, u32[]{:S(2)}) copy-start(bf16[704,128]{1,0:T(8,128)(2,1)} %param.19) | copy-start | bytes 540676
  107.0 50.3 %all-to-all-start.3 = ((bf16[16,704,128]{2,1,0:T(8,128)(2,1)}), bf16[16,704,128]{2,1,0:T(8,128)(2,1)}, u32[]{:S(2)}, u32[]{:S(2)}) async-start(bf16[16,704,128]{2,1,0:T(8,128)(2,1)} %broadcast_in_dim.55), calls=%async_computation.3 | async-start | bytes 5767168 | tf_op jit(solution)/shard_map/all_to_all | solution.py:20
  111.5 88.5 %reduce-scatter.2.cloned.1.call-start = ((), (), s32[]{:S(2)}) async-start(), calls=%async_computation.6 | async-start | bytes 4718592 | tf_op jit(solution)/shard_map/reduce_scatter | solution.py:133
  111.7 2.2 %copy-start.1 = (bf16[512,512,4]{0,2,1:T(4,128)(2,1)S(1)}, bf16[512,512,4]{0,2,1:T(4,128)(2,1)}, u32[]{:S(2)}) copy-start(bf16[512,512,4]{0,2,1:T(4,128)(2,1)} %reshape.114) | copy-start | bytes 6291460
  120.0 5.3 %copy-start.7 = (f32[2048]{0:T(1024)S(1)}, f32[2048]{0:T(1024)}, u32[]{:S(2)}) copy-start(f32[2048]{0:T(1024)} %param.13) | copy-start | bytes 24580
  125.4 5.2 %copy-start.9 = (f32[2048]{0:T(1024)S(1)}, f32[2048]{0:T(1024)}, u32[]{:S(2)}) copy-start(f32[2048]{0:T(1024)} %param.14) | copy-start | bytes 24580
  128.1 1.3 copy-start.2
  130.0 0.6 copy-start.8
  130.0 7.4 %copy-start.3 = (bf16[512,2048]{0,1:T(8,128)(2,1)S(1)}, bf16[512,2048]{0,1:T(8,128)(2,1)}, u32[]{:S(2)}) copy-start(bf16[512,2048]{0,1:T(8,128)(2,1)} %copy-done.2) | copy-start | bytes 6291460
Sparse Core Ops, SparseCore 0:
  9.4 66.9 all-gather.1
  163.3 36.6 reduce-scatter.1
where the time goes:
time: 210 us; the launch traced here: 209 us
  waiting for transfers between devices  69.5 us (33%)
  other arithmetic  47.4 us (23%)
  local copies, waits for them, and re-layouts  39.8 us (19%)
  starting transfers between devices  21.7 us (10%)
  matrix products  16.7 us (8%)
  between operations  13.6 us (6%)
    reduce_scatter x1, waiting for transfers between devices, body(): lax.psum_scatter(partial_value, 'tp', scatter_dimension=1, tiled=True)  36.8 us
    all_to_all x4, waiting for transfers between devices, from_everyone(): return lax.all_to_all(copies, axis, split_axis=0, concat_axis=0, tiled=True)  32.6 us
    all_to_all x4, starting transfers between devices, from_everyone(): return lax.all_to_all(copies, axis, split_axis=0, concat_axis=0, tiled=True)  21.4 us
    convert_element_type x1, other arithmetic, body(): pool_less(normed.astype(jnp.float32).reshape(seq_count, LEN, channels))  16.9 us
    convert_element_type x1, other arithmetic, body(): (jax.nn.silu(gate_conv) * value_conv).astype(jnp.bfloat16)  10.6 us
    add x3, other arithmetic, pool_less(): running = running + delayed(running, amount)  10.2 us
    dot_general x2, matrix products, add_rows(): return jnp.dot(left, portion, preferred_element_type=jnp.float32)  9.57 us
    broadcast_in_dim x4, local copies, waits for them, and re-layouts, from_everyone(): copies = jnp.broadcast_to(shard, (lax.axis_size(axis), *shard.shape))  6.13 us
  transfers between devices with their start and end apart: 6, of which 4 were waited for; matrix products, arithmetic and copies ran while one was open for 44% of the time, Pallas kernels for 0%

commit v1 on v0

v1 whole, which is shorter than its diff:
```python
import jax
import jax.numpy as jnp
from jax import lax
from jax.experimental import pallas as pl
from jax.experimental.pallas import tpu as pltpu
from jax.sharding import PartitionSpec as P

MESH = pl.DeviceIdType.MESH
bf16, f32 = jnp.bfloat16, jnp.float32
EPS = 1e-6
LEN = 128
TOK = 256


def concat(parts, axis):
    return jnp.concatenate(parts, axis=axis)


def iota(shape, dim):
    return lax.broadcasted_iota(jnp.int32, shape, dim)


def kernel(
    stream, gain_mix, pool_weight, pool_gain, gain_ffn, gate_weight, up_weight, gate_taps, up_taps,
    down_weight,
    out,
    gu, dn, pw, xs, sv, gwv, uwv, pv, gv, tv, taps, perm, unperm, band, gains, xg, wg, nf, acc, hid,
    pb, rbuf,
    lsem, gsem, dsem, psem, gd, dd, pys, pds, xys, xds, rsem, ssem,
):
    fs, tp = lax.axis_index("fs"), lax.axis_index("tp")
    z, x = fs // 4, fs % 4
    y, c = tp // 2, tp % 2

    def at_fs(dx, dz):
        return ((z + dz + 4) % 4) * 4 + (x + dx + 4) % 4

    def at_y(dy, core):
        return ((y + dy + 4) % 4) * 2 + core

    partner = (fs, y * 2 + (1 - c))

    barrier = pltpu.get_barrier_semaphore()
    peers = [(at_fs(1, 0), tp), (at_fs(-1, 0), tp), (at_fs(0, 1), tp), (at_fs(0, -1), tp)]
    peers += [(fs, (tp + d) % 8) for d in range(1, 8)]
    for peer in peers:
        pl.semaphore_signal(barrier, inc=1, device_id=peer, device_id_type=MESH)

    loads = [
        (gate_weight, gwv),
        (up_weight, uwv),
        (pool_weight, pv),
        (down_weight, dn.at[c, fs]),
        (stream.at[pl.ds(pl.multiple_of(c * TOK, TOK), TOK)], xs.at[y, c]),
        (stream.at[pl.ds(pl.multiple_of((1 - c) * TOK, TOK), TOK)], sv),
        (gain_mix, gv.at[0]),
        (pool_gain, gv.at[1]),
        (gain_ffn, gv.at[2]),
        (gate_taps.at[:, pl.ds(pl.multiple_of(y * 1408, 128), 1408)], tv.at[0]),
        (up_taps.at[:, pl.ds(pl.multiple_of(y * 1408, 128), 1408)], tv.at[1]),
    ]
    loads = [pltpu.make_async_copy(a, b, lsem.at[i]) for i, (a, b) in enumerate(loads)]
    for load in loads:
        load.start()
    for load in loads[:3]:
        load.wait()
    gu[c, fs, :, 0:640] = gwv[:, 0:640]
    gu[c, fs, :, 640:768] = concat([gwv[:, 640:704], uwv[:, 640:704]], 1)
    gu[c, fs, :, 768:1408] = uwv[:, 0:640]
    for p in range(2):
        pw[tp, fs, 32 * p : 32 * p + 32, :] = concat([pv[2 * p], pv[2 * p + 1]], 1)
    for load in loads[3:]:
        load.wait()
    pl.semaphore_wait(barrier, len(peers))

    def remote(src, dst, send, recv, device):
        return pltpu.make_async_remote_copy(
            src_ref=src, dst_ref=dst, send_sem=send, recv_sem=recv, device_id=device,
            device_id_type=MESH,
        )

    class Tree:
        def __init__(self, block, rows, recv, send):
            self.block, self.rows, self.recv, self.send = block, rows, recv, send

        def ref(self, q, a, b):
            color, sign = q // 2, 1 - 2 * (q % 2)
            j = at_fs(-sign * (a * (1 - color) + b * color), -sign * (a * color + b * (1 - color)))
            rows = pl.ds(pl.multiple_of(q * self.rows, self.rows), self.rows)
            return self.block(j).at[rows]

        def push(self, q, a, b, da, db):
            color, sign = q // 2, 1 - 2 * (q % 2)
            to = at_fs(sign * (da * (1 - color) + db * color), sign * (da * color + db * (1 - color)))
            ref = self.ref(q, a, b)
            pos = ((a + da) % 4) * 4 + (b + db) % 4
            remote(ref, ref, self.send, self.recv.at[q, pos], (to, tp)).start()

        def await_(self, q, a, b):
            ref = self.ref(q, a, b)
            pltpu.make_async_copy(ref, ref, self.recv.at[q, (a % 4) * 4 + b % 4]).wait()

        def each(self, f):
            def go(q, carry):
                f(q)
                return carry

            lax.fori_loop(0, 4, go, 0)

        def own(self):
            def f(q):
                self.push(q, 0, 0, 1, 0)
                self.push(q, 0, 0, -1, 0)
                self.push(q, 0, 0, 0, 1)
                self.push(q, 0, 0, 0, -1)

            self.each(f)

        def first(self):
            def f(q):
                self.await_(q, 1, 0)
                self.push(q, 1, 0, 1, 0)
                self.push(q, 1, 0, 0, 1)
                self.push(q, 1, 0, 0, -1)
                self.await_(q, -1, 0)
                self.push(q, -1, 0, 0, 1)
                self.push(q, -1, 0, 0, -1)

            self.each(f)

        def second(self):
            def f(q):
                self.await_(q, 2, 0)
                self.push(q, 2, 0, 0, 1)
                self.push(q, 2, 0, 0, -1)

            self.each(f)

        def cross(self, a):
            def f(q):
                self.await_(q, a, 1)
                self.push(q, a, 1, 0, 1)
                self.await_(q, a, -1)

            self.each(f)

        def end(self, a):
            self.each(lambda q: self.await_(q, a, 2))

    pool = Tree(lambda j: pw.at[tp, j], 16, psem, ssem.at[0])
    gup = Tree(lambda j: gu.at[c, j], 32, gsem, ssem.at[1])
    down = Tree(lambda j: dn.at[c, j], 176, dsem, ssem.at[2])

    def across(blocks, recv, send, offsets):
        for dx, dz in offsets:
            j, pos = at_fs(dx, dz), (dx % 4) * 4 + dz % 4
            remote(blocks.at[c, j], blocks.at[c, j], send, recv.at[pos], partner).start()

    def across_wait(blocks, recv, offsets):
        for dx, dz in offsets:
            j, pos = at_fs(dx, dz), (dx % 4) * 4 + dz % 4
            ref = blocks.at[1 - c, j]
            pltpu.make_async_copy(ref, ref, recv.at[pos]).wait()

    NEAR = [(1, 0), (-1, 0), (0, 1), (0, -1)]
    FAR = [(2, 0), (0, 2)]
    DIAG = [(1, 1), (1, -1), (-1, 1), (-1, -1)]
    KNIGHT = [(2, 1), (2, -1), (1, 2), (-1, 2)]
    ALL = [(0, 0)] + NEAR + FAR + DIAG + KNIGHT + [(2, 2)]

    def piece(dy, p):
        return xs.at[(y + dy + 4) % 4, p]

    def piece_out(p):
        remote(piece(0, p), piece(0, p), ssem.at[3], xys.at[p, 0], (fs, at_y(1, c))).start()
        remote(piece(0, p), piece(0, p), ssem.at[3], xys.at[p, 1], (fs, at_y(-1, c))).start()

    def got(ref, sem):
        pltpu.make_async_copy(ref, ref, sem).wait()

    remote(sv, xs.at[y, c], ssem.at[4], xds.at[0], partner).start()
    pool.own()
    piece_out(c)
    gup.own()
    across(gu, gd, ssem.at[5], [(0, 0)])
    across(dn, dd, ssem.at[6], [(0, 0)])

    d, n = iota((512, 512), 0), iota((512, 512), 1)
    perm[...] = ((d % 4) * 128 + d // 4 == n).astype(bf16)
    unperm[...] = ((n % 4) * 128 + n // 4 == d).astype(bf16)
    row, col = iota((LEN, LEN), 0), iota((LEN, LEN), 1)
    for g in range(4):
        band[g] = ((col <= row) & (col > row - 2 ** (g + 1))).astype(bf16)

    got(xs.at[y, 1 - c], xds.at[0])
    piece_out(1 - c)
    pool.first()
    pool.second()
    gup.first()

    three = concat([gv[0], gv[1], gv[2], jnp.zeros((5, 2048), f32)], 0)
    high = three.astype(bf16)
    rest = three - high.astype(f32)
    mid = rest.astype(bf16)
    low = (rest - mid.astype(f32)).astype(bf16)
    for yy in range(4):
        s = slice(512 * yy, 512 * yy + 512)
        moved = sum(jnp.dot(v[:, s], perm[...], preferred_element_type=f32) for v in (low, mid, high))
        for g in range(4):
            gains[g, :, 128 * yy : 128 * yy + 128] = moved[:, 128 * g : 128 * g + 128]
    for core in range(2):
        a = 704 * core
        gt, ut = tv[0, :, a : a + 704], tv[1, :, a : a + 704]
        taps[core, :, 0:640] = gt[:, 0:640]
        taps[core, :, 640:768] = concat([gt[:, 640:704], ut[:, 640:704]], 1)
        taps[core, :, 768:1408] = ut[:, 0:640]

    pool.cross(0)
    gup.second()
    pool.cross(1)
    pool.cross(-1)
    pool.cross(2)
    gup.cross(0)
    across(gu, gd, ssem.at[5], NEAR)
    for a in (0, 1, -1, 2):
        pool.end(a)

    def columns(dy, core):
        return pw.at[at_y(dy, core)]

    def pool_across(i, dy):
        remote(columns(dy, c), columns(dy, c), ssem.at[7], pds.at[i], partner).start()

    remote(columns(0, c), columns(0, c), ssem.at[8], pys.at[0], (fs, at_y(1, c))).start()
    remote(columns(0, c), columns(0, c), ssem.at[8], pys.at[1], (fs, at_y(-1, c))).start()
    pool_across(0, 0)

    got(piece(-1, 0), xys.at[0, 0])
    remote(piece(-1, 0), piece(-1, 0), ssem.at[3], xys.at[0, 2], (fs, at_y(1, c))).start()
    got(piece(1, 1), xys.at[1, 1])
    remote(piece(1, 1), piece(1, 1), ssem.at[3], xys.at[1, 2], (fs, at_y(-1, c))).start()
    got(piece(1, 0), xys.at[0, 1])
    got(piece(-1, 1), xys.at[1, 0])

    acc[...] = jnp.zeros_like(acc)

    def regroup(yy, carry):
        xp = jnp.dot(concat([xs[yy, 0], xs[yy, 1]], 1), perm[...], preferred_element_type=f32)
        at = pl.ds(pl.multiple_of(yy * 128, 128), 128)
        total = acc[...]
        for g in range(4):
            part = xp[:, 128 * g : 128 * g + 128]
            xg[g, :, at] = part.astype(bf16)
            total = total + part * part
        acc[...] = total
        return carry

    regroup(y, 0)
    gup.cross(1)
    regroup((y + 1) % 4, 0)
    gup.cross(-1)
    regroup((y + 3) % 4, 0)
    across(gu, gd, ssem.at[5], DIAG)
    gup.end(0)
    across(gu, gd, ssem.at[5], FAR)
    gup.cross(2)
    down.own()
    got(piece(2, 0), xys.at[0, 2])
    got(piece(2, 1), xys.at[1, 2])
    regroup((y + 2) % 4, 0)

    got(columns(-1, c), pys.at[0])
    half = columns(-1, c).at[0:8]
    remote(half, half, ssem.at[8], pys.at[2], (fs, at_y(1, c))).start()
    pool_across(1, -1)
    got(columns(1, c), pys.at[1])
    half = columns(1, c).at[8:16]
    remote(half, half, ssem.at[8], pys.at[3], (fs, at_y(-1, c))).start()
    pool_across(2, 1)

    def unpack(yy, carry):
        at = pl.ds(pl.multiple_of(yy * 128, 128), 128)
        for p in range(2):
            left = pw[2 * yy, :, 32 * p : 32 * p + 32, :].reshape(512, 128)
            right = pw[2 * yy + 1, :, 32 * p : 32 * p + 32, :].reshape(512, 128)
            wg[2 * p, :, at] = concat([left[:, 0:64], right[:, 0:64]], 1)
            wg[2 * p + 1, :, at] = concat([left[:, 64:128], right[:, 64:128]], 1)
        return carry

    got(columns(0, 1 - c), pds.at[0])
    unpack(y, 0)
    gup.end(1)
    gup.end(-1)
    got(columns(2, c).at[0:8], pys.at[2])
    got(columns(2, c).at[8:16], pys.at[3])
    pool_across(3, 2)
    got(columns(-1, 1 - c), pds.at[1])
    unpack((y + 3) % 4, 0)
    got(columns(1, 1 - c), pds.at[2])
    unpack((y + 1) % 4, 0)
    across(gu, gd, ssem.at[5], KNIGHT)
    gup.end(2)
    across(gu, gd, ssem.at[5], [(2, 2)])
    got(columns(2, 1 - c), pds.at[3])
    unpack((y + 2) % 4, 0)

    scale = lax.rsqrt(jnp.sum(acc[...], axis=1, keepdims=True) * (1.0 / 2048) + EPS)
    acc[...] = jnp.zeros_like(acc)
    position = iota((LEN, 512), 0) + 1

    def mix(g, carry):
        divisor = jnp.minimum(position, lax.shift_left(2, g)).astype(f32)
        normed = (xg[g].astype(f32) * scale * gains[g, 0:1, :]).astype(bf16)
        pooled = []
        for s in range(TOK // LEN):
            part = normed[LEN * s : LEN * s + LEN]
            window = jnp.dot(band[g], part, preferred_element_type=f32)
            pooled.append((window / divisor - part.astype(f32)).astype(bf16))
        mixer = jnp.dot(concat(pooled, 0), wg[g], preferred_element_type=f32) * gains[g, 1:2, :]
        middle = (xg[g].astype(f32) + mixer).astype(bf16)
        xg[g] = middle
        total = acc[...]
        for i in range(4):
            part = middle[:, 128 * i : 128 * i + 128].astype(f32)
            total = total + part * part
        acc[...] = total
        return carry

    lax.fori_loop(0, 4, mix, 0)
    down.first()
    scale = lax.rsqrt(jnp.sum(acc[...], axis=1, keepdims=True) * (1.0 / 2048) + EPS)

    def rescale(g, carry):
        xg[g] = (xg[g].astype(f32) * scale * gains[g, 2:3, :]).astype(bf16)
        return carry

    lax.fori_loop(0, 4, rescale, 0)

    def natural(yy, carry):
        at = pl.ds(pl.multiple_of(yy * 128, 128), 128)
        grouped = concat([xg[g, :, at] for g in range(4)], 1)
        moved = jnp.dot(grouped, unperm[...], preferred_element_type=f32).astype(bf16)
        nf[:, pl.ds(pl.multiple_of(yy * 512, 512), 512)] = moved
        return carry

    lax.fori_loop(0, 4, natural, 0)
    down.second()

    place = iota((TOK, 128), 0) % LEN

    def conv(core, at, width):
        block = gu[core, :, :, at : at + width].reshape(2048, width)
        v = jnp.dot(nf[...], block, preferred_element_type=f32).astype(bf16).astype(f32)
        outs = []
        for i in range(width // 128):
            part = v[:, 128 * i : 128 * i + 128]
            k = taps[core, :, at + 128 * i : at + 128 * i + 128]
            back1 = jnp.where(place >= 1, pltpu.roll(part, 1, 0), 0.0)
            back2 = jnp.where(place >= 2, pltpu.roll(part, 2, 0), 0.0)
            outs.append(back2 * k[0:1] + back1 * k[1:2] + part * k[2:3])
        return outs

    def gated(a, b):
        return (a / (1.0 + jnp.exp(-a)) * b).astype(bf16)

    def units(core, t):
        for i, (a, b) in enumerate(zip(conv(core, 256 * t, 256), conv(core, 768 + 256 * t, 256))):
            at = 256 * t + 128 * i
            hid[core, :, at : at + 128] = gated(a, b)

    def last_units(core):
        a, both = conv(core, 512, 256)
        (b,) = conv(core, 1280, 128)
        hid[core, :, 512:640] = gated(a, b)
        hid[core, :, 640:704] = gated(both[:, 0:64], both[:, 64:128])

    units(c, 0)
    down.cross(0)
    across(dn, dd, ssem.at[6], NEAR)
    units(c, 1)
    down.end(0)
    across(dn, dd, ssem.at[6], FAR)
    last_units(c)
    down.cross(1)
    down.cross(-1)
    across(dn, dd, ssem.at[6], DIAG)
    across_wait(gu, gd, ALL)
    units(1 - c, 0)
    down.cross(2)
    units(1 - c, 1)
    last_units(1 - c)

    def owner_columns(dz, other):
        xpair = x // 2 if other == 0 else 1 - x // 2
        zk = (z + dz + 4) % 4
        k = zk * 2 + xpair
        total = None
        for core in range(2):
            block = concat([dn[core, 2 * k], dn[core, 2 * k + 1]], 1)
            part = jnp.dot(hid[core], block, preferred_element_type=f32)
            total = part if total is None else total + part
        pb[k] = total.astype(bf16)
        own = k == tp

        @pl.when(own)
        def _():
            rbuf[tp] = total.astype(bf16)

        @pl.when(jnp.logical_not(own))
        def _():
            remote(pb.at[k], rbuf.at[tp], ssem.at[9], rsem.at[tp], (fs, k)).start()

    down.end(1)
    down.end(-1)
    across(dn, dd, ssem.at[6], KNIGHT)
    down.end(2)
    across(dn, dd, ssem.at[6], [(2, 2)])
    across_wait(dn, dd, ALL)
    for dz in (0, 1, -1, 2):
        for other in (0, 1):
            owner_columns(dz, other)

    for i in range(1, 8):
        src = (tp + i) % 8
        got(rbuf.at[src], rsem.at[src])
    for core in range(2):
        total = rbuf[core].astype(f32)
        for yy in range(1, 4):
            total = total + rbuf[2 * yy + core].astype(f32)
        out[TOK * core : TOK * core + TOK, :] = total.astype(bf16)

    for ref, i in (
        (pw.at[0, 0:15], 0), (gu.at[0, 0:15], 1), (dn.at[0, 0:15], 2), (xs.at[0:3], 3), (sv, 4),
        (gu.at[0], 5), (dn.at[0], 6), (pw.at[0:4], 7), (pw.at[0:3], 8), (pb.at[0:7], 9),
    ):
        got(ref, ssem.at[i])


def body(
    stream, gain_mix, pool_weight, pool_gain, gain_ffn, gate_weight, up_weight, gate_taps, up_taps,
    down_weight,
):
    row = lambda v: v.reshape(1, 2048)
    DMA = pltpu.SemaphoreType.DMA
    return pl.pallas_call(
        kernel,
        name="layer",
        out_shape=jax.ShapeDtypeStruct((512, 256), bf16),
        in_specs=[pl.BlockSpec(memory_space=pl.ANY)] * 10,
        out_specs=pl.BlockSpec(memory_space=pltpu.VMEM),
        scratch_shapes=[
            pltpu.VMEM((2, 16, 128, 1408), bf16),
            pltpu.VMEM((2, 16, 704, 128), bf16),
            pltpu.VMEM((8, 16, 64, 128), bf16),
            pltpu.VMEM((4, 2, TOK, 256), bf16),
            pltpu.VMEM((TOK, 256), bf16),
            pltpu.VMEM((128, 704), bf16),
            pltpu.VMEM((128, 704), bf16),
            pltpu.VMEM((4, 32, 64), bf16),
            pltpu.VMEM((3, 1, 2048), f32),
            pltpu.VMEM((2, 3, 1408), f32),
            pltpu.VMEM((2, 3, 1408), f32),
            pltpu.VMEM((512, 512), bf16),
            pltpu.VMEM((512, 512), bf16),
            pltpu.VMEM((4, LEN, LEN), bf16),
            pltpu.VMEM((4, 8, 512), f32),
            pltpu.VMEM((4, TOK, 512), bf16),
            pltpu.VMEM((4, 512, 512), bf16),
            pltpu.VMEM((TOK, 2048), bf16),
            pltpu.VMEM((TOK, 128), f32),
            pltpu.VMEM((2, TOK, 704), bf16),
            pltpu.VMEM((8, TOK, 256), bf16),
            pltpu.VMEM((8, TOK, 256), bf16),
            DMA((11,)),
            DMA((4, 16)),
            DMA((4, 16)),
            DMA((4, 16)),
            DMA((16,)),
            DMA((16,)),
            DMA((4,)),
            DMA((4,)),
            DMA((2, 3)),
            DMA((1,)),
            DMA((8,)),
            DMA((10,)),
        ],
        compiler_params=pltpu.CompilerParams(
            collective_id=0, has_side_effects=True, vmem_limit_bytes=60 * 1024 * 1024
        ),
    )(
        stream, row(gain_mix), pool_weight, row(pool_gain), row(gain_ffn), gate_weight, up_weight,
        gate_taps, up_taps, down_weight,
    )


def solution(mesh):
    return jax.shard_map(
        body,
        mesh=mesh,
        in_specs=(
            P("fs", "tp"), P(), P(None, "fs", "tp"), P(), P(), P("fs", "tp"), P("fs", "tp"), P(), P(),
            P("tp", "fs"),
        ),
        out_specs=P("fs", "tp"),
        check_vma=False,
    )
```

time: 210 us -> 96.1 us (0.46)
  the two profiles are of different devices: /device:TPU:0 before, /device:TPU:33 now
where the time goes in v1:
time: 96.1 us; the launch traced here: 95.1 us
  Pallas kernels  90.8 us (94%)
  local copies, waits for them, and re-layouts  4.27 us (4%)
    pallas_call x1, Pallas kernels, body(): pl.pallas_call(kernel, name='layer', out_shape=jax.ShapeDtypeStruct((512,...  90.8 us
    unnamed x5, local copies, waits for them, and re-layouts  4.27 us

profile of v1, /device:TPU:33, one launch (start us, length us, event | category | flops | bytes accessed | tf_op | source)
XLA Modules:
  0.0 95.1 jit_solution(9267071136290447308)
XLA Ops:
  0.0 0.0 copy-start
  0.0 1.8 %copy.11.gate_weight = bf16[128,704]{1,0:T(8,128)(2,1)} copy(bf16[128,704]{0,1:T(8,128)(2,1)} %param.15) | data formatting | bytes 360448 | tf_op args[5]
  1.8 0.0 copy-done
  1.8 0.8 copy.12.up_weight
  2.6 90.8 %layer.1 = bf16[512,256]{1,0:T(8,128)(2,1)} custom-call(bf16[512,256]{1,0:T(8,128)(2,1)} %stream.1, f32[1,2048]{1,0:T(1,128)} %bitcast.3, bf16[4,32,64]{2,1,0:T(8,128)(2,1)} %pool_weight.1, f32[1,2048]{1,0:T(1,128)} %bitcast.4, f32[1,2048]{1,0:T(1,128)} %bitcast.5, bf16[128,704]{1,0:T(8,128)(2,1)} %copy.11.gate_weight, bf16[128,704]{1,0:T(8,128)(2,1)} %copy.12.up_weight, ...), custom_call_target="tpu_custom_call" | custom-call | tf_op jit(solution)/shard_map/layer/pallas_call | solution.py:445
  93.4 1.7 %copy.14 = bf16[512,256]{1,0:T(8,128)(2,1)} copy(bf16[512,256]{1,0:T(8,128)(2,1)} %layer.1) | data formatting | bytes 524288
Async XLA Ops:
  0.0 1.8 %copy-start = (bf16[128,704]{0,1:T(8,128)(2,1)S(1)}, bf16[128,704]{0,1:T(8,128)(2,1)}, u32[]{:S(2)}) copy-start(bf16[128,704]{0,1:T(8,128)(2,1)} %param.16) | copy-start | bytes 540676

commit v2 on v1

v2 whole, which is shorter than its diff:
```python
import jax
import jax.numpy as jnp
from jax import lax
from jax.experimental import pallas as pl
from jax.experimental.pallas import tpu as pltpu
from jax.sharding import PartitionSpec as P

MESH = pl.DeviceIdType.MESH
bf16, f32 = jnp.bfloat16, jnp.float32
EPS = 1e-6
LEN = 128
TOK = 256


def concat(parts, axis):
    return jnp.concatenate(parts, axis=axis)


def iota(shape, dim):
    return lax.broadcasted_iota(jnp.int32, shape, dim)


def kernel(
    stream, gain_mix, pool_weight, pool_gain, gain_ffn, gate_weight, up_weight, gate_taps, up_taps,
    down_weight,
    out,
    gu, dn, pw, xs, sv, pv, gv, tv, taps, perm, unperm, band, gains, xg, wg, nf, acc, hid,
    pb, rbuf, sums, relay_in,
    lsem, gsem, dsem, psem, gd, dd, pys, pds, xys, xds, rsem, ssem, relsem,
):
    fs, tp = lax.axis_index("fs"), lax.axis_index("tp")
    z, x = fs // 4, fs % 4
    y, c = tp // 2, tp % 2

    def at_fs(dx, dz):
        return ((z + dz + 4) % 4) * 4 + (x + dx + 4) % 4

    def at_y(dy, core):
        return ((y + dy + 4) % 4) * 2 + core

    partner = (fs, y * 2 + (1 - c))

    barrier = pltpu.get_barrier_semaphore()
    others = [(dx, dz) for dz in (0, 1, -1, 2) for dx in (0, 1, -1, 2)][1:]
    peers = [(at_fs(dx, dz), tp) for dx, dz in others]
    peers += [(fs, at_y(dy, core)) for dy in (1, -1) for core in (0, 1)] + [partner]
    for peer in peers:
        pl.semaphore_signal(barrier, inc=1, device_id=peer, device_id_type=MESH)

    loads = [
        (pool_weight, pv),
        (gate_weight, gu.at[c, fs, pl.ds(0, 704)]),
        (up_weight, gu.at[c, fs, pl.ds(704, 704)]),
        (down_weight, dn.at[c, fs]),
        (stream.at[pl.ds(pl.multiple_of(c * TOK, TOK), TOK)], xs.at[y, c]),
        (stream.at[pl.ds(pl.multiple_of((1 - c) * TOK, TOK), TOK)], sv),
        (gain_mix, gv.at[0]),
        (pool_gain, gv.at[1]),
        (gain_ffn, gv.at[2]),
        (gate_taps.at[:, pl.ds(pl.multiple_of(y * 1408, 128), 1408)], tv.at[0]),
        (up_taps.at[:, pl.ds(pl.multiple_of(y * 1408, 128), 1408)], tv.at[1]),
    ]
    loads = [pltpu.make_async_copy(a, b, lsem.at[i]) for i, (a, b) in enumerate(loads)]
    for load in loads:
        load.start()
    loads[0].wait()
    for p in range(2):
        pw[tp, fs, 32 * p : 32 * p + 32, :] = concat([pv[2 * p], pv[2 * p + 1]], 1)
    for load in loads[1:]:
        load.wait()
    pl.semaphore_wait(barrier, len(peers))

    def remote(src, dst, send, recv, device):
        return pltpu.make_async_remote_copy(
            src_ref=src, dst_ref=dst, send_sem=send, recv_sem=recv, device_id=device,
            device_id_type=MESH,
        )

    class Tree:
        def __init__(self, block, rows, recv, send):
            self.block, self.rows, self.recv, self.send = block, rows, recv, send

        def ref(self, q, a, b):
            color, sign = q // 2, 1 - 2 * (q % 2)
            j = at_fs(-sign * (a * (1 - color) + b * color), -sign * (a * color + b * (1 - color)))
            rows = pl.ds(pl.multiple_of(q * self.rows, self.rows), self.rows)
            return self.block(j).at[rows]

        def push(self, q, a, b, da, db):
            color, sign = q // 2, 1 - 2 * (q % 2)
            to = at_fs(sign * (da * (1 - color) + db * color), sign * (da * color + db * (1 - color)))
            ref = self.ref(q, a, b)
            pos = ((a + da) % 4) * 4 + (b + db) % 4
            remote(ref, ref, self.send, self.recv.at[pos], (to, tp)).start()

        def await_(self, a, b):
            ref = self.block(fs)
            pltpu.make_async_copy(ref, ref, self.recv.at[(a % 4) * 4 + b % 4]).wait()

        def each(self, f):
            def go(q, carry):
                f(q)
                return carry

            lax.fori_loop(0, 4, go, 0)

        def run(self, *items):
            for a, b, wait, steps in items:
                if wait:
                    self.await_(a, b)

                def f(q):
                    for da, db in steps:
                        self.push(q, a, b, da, db)

                if steps:
                    self.each(f)

    gup = Tree(lambda j: gu.at[c, j], 352, gsem, ssem.at[1])
    down = Tree(lambda j: dn.at[c, j], 176, dsem, ssem.at[2])

    def across(blocks, recv, send, offsets):
        for dx, dz in offsets:
            j, pos = at_fs(dx, dz), (dx % 4) * 4 + dz % 4
            remote(blocks.at[c, j], blocks.at[c, j], send, recv.at[pos], partner).start()

    def across_wait(blocks, recv, offsets):
        for dx, dz in offsets:
            j, pos = at_fs(dx, dz), (dx % 4) * 4 + dz % 4
            ref = blocks.at[1 - c, j]
            pltpu.make_async_copy(ref, ref, recv.at[pos]).wait()

    NEAR = [(1, 0), (-1, 0), (0, 1), (0, -1)]
    FAR = [(2, 0), (0, 2)]
    DIAG = [(1, 1), (1, -1), (-1, 1), (-1, -1)]
    KNIGHT = [(2, 1), (2, -1), (1, 2), (-1, 2)]
    ALL = [(0, 0)] + NEAR + FAR + DIAG + KNIGHT + [(2, 2)]

    def piece(dy, p):
        return xs.at[(y + dy + 4) % 4, p]

    def piece_out(p):
        remote(piece(0, p), piece(0, p), ssem.at[3], xys.at[p, 0], (fs, at_y(1, c))).start()
        remote(piece(0, p), piece(0, p), ssem.at[3], xys.at[p, 1], (fs, at_y(-1, c))).start()

    def got(ref, sem):
        pltpu.make_async_copy(ref, ref, sem).wait()

    RIGHT, LEFT, UP, DOWN = (1, 0), (-1, 0), (0, 1), (0, -1)
    remote(sv, xs.at[y, c], ssem.at[4], xds.at[0], partner).start()
    piece_out(c)
    for dx, dz in others:
        mine = pw.at[tp, fs]
        remote(mine, mine, ssem.at[0], psem.at[0], (at_fs(dx, dz), tp)).start()
    gup.run((0, 0, False, [RIGHT]))
    gup.run((0, 0, False, [UP]))
    gup.run((0, 0, False, [LEFT]))
    across(gu, gd, ssem.at[5], [(0, 0)])
    across(dn, dd, ssem.at[6], [(0, 0)])

    d, n = iota((512, 512), 0), iota((512, 512), 1)
    perm[...] = ((d % 4) * 128 + d // 4 == n).astype(bf16)
    unperm[...] = ((n % 4) * 128 + n // 4 == d).astype(bf16)
    row, col = iota((LEN, LEN), 0), iota((LEN, LEN), 1)
    for g in range(4):
        band[g] = ((col <= row) & (col > row - 2 ** (g + 1))).astype(bf16)

    got(xs.at[y, 1 - c], xds.at[0])
    piece_out(1 - c)

    three = concat([gv[0], gv[1], gv[2], jnp.zeros((5, 2048), f32)], 0)
    high = three.astype(bf16)
    rest = three - high.astype(f32)
    mid = rest.astype(bf16)
    low = (rest - mid.astype(f32)).astype(bf16)
    for yy in range(4):
        s = slice(512 * yy, 512 * yy + 512)
        moved = sum(jnp.dot(v[:, s], perm[...], preferred_element_type=f32) for v in (low, mid, high))
        for g in range(4):
            gains[g, :, 128 * yy : 128 * yy + 128] = moved[:, 128 * g : 128 * g + 128]
    for core in range(2):
        a = 704 * core
        taps[core, 0] = tv[0, :, a : a + 704]
        taps[core, 1] = tv[1, :, a : a + 704]

    gup.run((1, 0, True, [RIGHT]))
    gup.run((0, 0, False, [DOWN]))
    gup.run((1, 0, False, [UP]))
    got(pw.at[tp, 0:15], psem.at[0])

    def columns(dy, core):
        return pw.at[at_y(dy, core)]

    def pool_across(i, dy):
        remote(columns(dy, c), columns(dy, c), ssem.at[7], pds.at[i], partner).start()

    remote(columns(0, c), columns(0, c), ssem.at[8], pys.at[0], (fs, at_y(1, c))).start()
    remote(columns(0, c), columns(0, c), ssem.at[8], pys.at[1], (fs, at_y(-1, c))).start()
    pool_across(0, 0)
    gup.run((2, 0, True, [UP]))

    got(piece(-1, 0), xys.at[0, 0])
    remote(piece(-1, 0), piece(-1, 0), ssem.at[3], xys.at[0, 2], (fs, at_y(1, c))).start()
    got(piece(1, 1), xys.at[1, 1])
    remote(piece(1, 1), piece(1, 1), ssem.at[3], xys.at[1, 2], (fs, at_y(-1, c))).start()
    gup.run((-1, 0, True, [UP]))
    gup.run((0, 1, True, [UP]), (1, 0, False, [DOWN]), (2, 0, False, [DOWN]), (-1, 0, False, [DOWN]))

    acc[...] = jnp.zeros_like(acc)

    def regroup(yy, carry):
        xp = jnp.dot(concat([xs[yy, 0], xs[yy, 1]], 1), perm[...], preferred_element_type=f32)
        at = pl.ds(pl.multiple_of(yy * 128, 128), 128)
        total = acc[...]
        for g in range(4):
            part = xp[:, 128 * g : 128 * g + 128]
            xg[g, :, at] = part.astype(bf16)
            total = total + part * part
        acc[...] = total
        return carry

    def unpack(yy, carry):
        at = pl.ds(pl.multiple_of(yy * 128, 128), 128)
        for p in range(2):
            left = pw[2 * yy, :, 32 * p : 32 * p + 32, :].reshape(512, 128)
            right = pw[2 * yy + 1, :, 32 * p : 32 * p + 32, :].reshape(512, 128)
            wg[2 * p, :, at] = concat([left[:, 0:64], right[:, 0:64]], 1)
            wg[2 * p + 1, :, at] = concat([left[:, 64:128], right[:, 64:128]], 1)
        return carry

    got(piece(1, 0), xys.at[0, 1])
    got(piece(-1, 1), xys.at[1, 0])
    regroup(y, 0)
    gup.run((0, -1, True, []))
    across(gu, gd, ssem.at[5], NEAR)
    regroup((y + 1) % 4, 0)
    regroup((y + 3) % 4, 0)
    got(columns(0, 1 - c), pds.at[0])
    unpack(y, 0)
    got(columns(-1, c), pys.at[0])
    half = columns(-1, c).at[0:8]
    remote(half, half, ssem.at[8], pys.at[2], (fs, at_y(1, c))).start()
    pool_across(1, -1)
    got(columns(1, c), pys.at[1])
    half = columns(1, c).at[8:16]
    remote(half, half, ssem.at[8], pys.at[3], (fs, at_y(-1, c))).start()
    pool_across(2, 1)
    gup.run((1, 1, True, [UP]))
    down.run((0, 0, False, [RIGHT]))
    gup.run((2, 1, True, [UP]))
    down.run((0, 0, False, [UP]))
    gup.run((-1, 1, True, [UP]))
    down.run((0, 0, False, [LEFT]))
    down.run((0, 0, False, [DOWN]))
    got(piece(2, 0), xys.at[0, 2])
    got(piece(2, 1), xys.at[1, 2])
    regroup((y + 2) % 4, 0)
    got(columns(-1, 1 - c), pds.at[1])
    unpack((y + 3) % 4, 0)
    got(columns(1, 1 - c), pds.at[2])
    unpack((y + 1) % 4, 0)
    got(columns(2, c).at[0:8], pys.at[2])
    got(columns(2, c).at[8:16], pys.at[3])
    pool_across(3, 2)
    got(columns(2, 1 - c), pds.at[3])
    unpack((y + 2) % 4, 0)
    gup.run((0, 2, True, []))
    across(gu, gd, ssem.at[5], FAR)

    scale = lax.rsqrt(jnp.sum(acc[...], axis=1, keepdims=True) * (1.0 / 2048) + EPS)
    acc[...] = jnp.zeros_like(acc)
    position = iota((LEN, 512), 0) + 1

    def mix(g, carry):
        divisor = jnp.minimum(position, lax.shift_left(2, g)).astype(f32)
        normed = (xg[g].astype(f32) * scale * gains[g, 0:1, :]).astype(bf16)
        pooled = []
        for s in range(TOK // LEN):
            part = normed[LEN * s : LEN * s + LEN]
            window = jnp.dot(band[g], part, preferred_element_type=f32)
            pooled.append((window / divisor - part.astype(f32)).astype(bf16))
        mixer = jnp.dot(concat(pooled, 0), wg[g], preferred_element_type=f32) * gains[g, 1:2, :]
        middle = (xg[g].astype(f32) + mixer).astype(bf16)
        xg[g] = middle
        total = acc[...]
        for i in range(4):
            part = middle[:, 128 * i : 128 * i + 128].astype(f32)
            total = total + part * part
        acc[...] = total
        return carry

    lax.fori_loop(0, 4, mix, 0)
    scale = lax.rsqrt(jnp.sum(acc[...], axis=1, keepdims=True) * (1.0 / 2048) + EPS)

    def rescale(g, carry):
        xg[g] = (xg[g].astype(f32) * scale * gains[g, 2:3, :]).astype(bf16)
        return carry

    lax.fori_loop(0, 4, rescale, 0)

    def natural(yy, carry):
        at = pl.ds(pl.multiple_of(yy * 128, 128), 128)
        grouped = concat([xg[g, :, at] for g in range(4)], 1)
        moved = jnp.dot(grouped, unperm[...], preferred_element_type=f32).astype(bf16)
        for i in range(4):
            nf[4 * yy + i] = moved[:, 128 * i : 128 * i + 128]
        return carry

    lax.fori_loop(0, 4, natural, 0)

    SETS = ([(0, 0)] + NEAR, FAR + DIAG, KNIGHT + [(2, 2)])
    CHUNKS = ((0, 256), (256, 256), (512, 192))

    def product(core, which, at, width, offsets):
        js = [at_fs(dx, dz) for dx, dz in offsets]
        left = concat([nf[j] for j in js], 1)
        right = concat([gu[core, j, pl.ds(704 * which + at, width), :] for j in js], 1)
        return lax.dot_general(left, right, (((1,), (1,)), ((), ())), preferred_element_type=f32)

    def gather_up(core, i):
        for which in range(2):
            for at, width in CHUNKS:
                part = product(core, which, at, width, SETS[i])
                if i > 0:
                    part = sums[core, which, :, at : at + width] + part
                sums[core, which, :, at : at + width] = part

    def conv(core, which, at, width):
        v = sums[core, which, :, at : at + width] + product(core, which, at, width, SETS[2])
        v = v.astype(bf16).astype(f32)
        k = taps[core, which, :, at : at + width]
        place = iota((TOK, width), 0) % LEN
        back1 = jnp.where(place >= 1, pltpu.roll(v, 1, 0), 0.0)
        back2 = jnp.where(place >= 2, pltpu.roll(v, 2, 0), 0.0)
        return back2 * k[0:1] + back1 * k[1:2] + v * k[2:3]

    def units(core, t):
        at, width = CHUNKS[t]
        a, b = conv(core, 0, at, width), conv(core, 1, at, width)
        hid[core, :, at : at + width] = (a / (1.0 + jnp.exp(-a)) * b).astype(bf16)

    gather_up(c, 0)
    across_wait(gu, gd, SETS[0])
    gather_up(1 - c, 0)
    gup.run((1, -1, True, []), (-1, -1, True, []), (2, -1, True, []))
    across(gu, gd, ssem.at[5], DIAG)
    gather_up(c, 1)
    across_wait(gu, gd, SETS[1])
    gather_up(1 - c, 1)
    down.run((1, 0, True, [RIGHT, UP]))
    gup.run((1, 2, True, []), (2, 2, True, []))
    down.run((0, 1, True, [UP]))
    gup.run((-1, 2, True, []))
    across(gu, gd, ssem.at[5], KNIGHT + [(2, 2)])
    units(c, 0)
    down.run((-1, 0, True, [UP, DOWN]), (1, 0, False, [DOWN]))
    units(c, 1)
    down.run((0, -1, True, []))
    across(dn, dd, ssem.at[6], NEAR)
    units(c, 2)
    down.run((2, 0, True, [UP, DOWN]))
    across_wait(gu, gd, SETS[2])
    units(1 - c, 0)
    down.run((1, 1, True, [UP]))
    units(1 - c, 1)
    down.run((-1, 1, True, [UP]))
    units(1 - c, 2)

    way = {(0, 0): 1, (0, 1): -1, (1, 0): -1, (1, 1): 1, (-1, 0): 1, (-1, 1): -1, (2, 0): 1, (2, 1): -1}

    def pair_of(dz, other):
        cols = x // 2 if other == 0 else 1 - x // 2
        zk = (z + dz + 4) % 4
        return zk * 2 + cols, cols, (zk - y + 4) % 4

    def to_owner(k, dy, cols):
        slot = 1 if dy == 1 else 2
        device = (fs, at_y(dy, cols))
        remote(pb.at[k], rbuf.at[slot, c], ssem.at[9], rsem.at[slot, c], device).start()

    def owner_columns(dz, other):
        k, cols, role = pair_of(dz, other)
        dy = way[dz, other]
        total = None
        for core in range(2):
            block = concat([dn[core, 2 * k], dn[core, 2 * k + 1]], 1)
            part = jnp.dot(hid[core], block, preferred_element_type=f32)
            total = part if total is None else total + part
        pb[k] = total.astype(bf16)

        @pl.when((role == 0) & (cols == c))
        def _():
            rbuf[0, c] = pb[k]

        @pl.when((role == 0) & (cols != c))
        def _():
            remote(pb.at[k], rbuf.at[0, c], ssem.at[9], rsem.at[0, c], partner).start()

        @pl.when(role == (3 if dy == 1 else 1))
        def _():
            to_owner(k, -dy, cols)

        @pl.when(role == 2)
        def _():
            slot = (1 - dy) // 2
            device = (fs, at_y(dy, c))
            remote(pb.at[k], relay_in.at[slot], ssem.at[9], relsem.at[slot], device).start()

    def owner_added(dz, other):
        k, cols, role = pair_of(dz, other)
        dy = way[dz, other]
        slot = (1 - dy) // 2

        @pl.when(role == (1 if dy == 1 else 3))
        def _():
            got(relay_in.at[slot], relsem.at[slot])
            pb[k] = (pb[k].astype(f32) + relay_in[slot].astype(f32)).astype(bf16)
            to_owner(k, dy, cols)

    across_wait(dn, dd, [(0, 0)] + NEAR)
    owner_columns(0, 0)
    down.run((0, 2, True, []))
    across(dn, dd, ssem.at[6], FAR)
    down.run((1, -1, True, []), (-1, -1, True, []), (2, -1, True, []))
    across(dn, dd, ssem.at[6], DIAG)
    across_wait(dn, dd, FAR)
    owner_columns(0, 1)
    down.run((2, 1, True, [UP]))
    owner_added(0, 0)
    down.run((1, 2, True, []), (-1, 2, True, []))
    across(dn, dd, ssem.at[6], KNIGHT)
    across_wait(dn, dd, DIAG)
    owner_columns(1, 0)
    owner_columns(-1, 0)
    down.run((2, 2, True, []))
    across(dn, dd, ssem.at[6], [(2, 2)])
    across_wait(dn, dd, KNIGHT)
    owner_columns(2, 0)
    owner_columns(1, 1)
    owner_added(0, 1)
    owner_columns(-1, 1)
    owner_added(1, 0)
    across_wait(dn, dd, [(2, 2)])
    owner_columns(2, 1)
    owner_added(-1, 0)
    owner_added(2, 0)
    owner_added(1, 1)
    owner_added(-1, 1)
    owner_added(2, 1)

    got(rbuf.at[1, 0], rsem.at[1, 0])
    got(rbuf.at[1, 1], rsem.at[1, 1])
    got(rbuf.at[2, 0], rsem.at[2, 0])
    got(rbuf.at[2, 1], rsem.at[2, 1])
    got(rbuf.at[0, 1 - c], rsem.at[0, 1 - c])
    for core in range(2):
        total = rbuf[0, core].astype(f32) + rbuf[1, core].astype(f32) + rbuf[2, core].astype(f32)
        out[TOK * core : TOK * core + TOK, :] = total.astype(bf16)

    for ref, i in (
        (pw.at[0, 0:15], 0), (gu.at[0, 0:15], 1), (dn.at[0, 0:15], 2), (xs.at[0:3], 3), (sv, 4),
        (gu.at[0], 5), (dn.at[0], 6), (pw.at[0:4], 7), (pw.at[0:3], 8), (pb.at[0:7], 9),
    ):
        got(ref, ssem.at[i])


def body(
    stream, gain_mix, pool_weight, pool_gain, gain_ffn, gate_weight, up_weight, gate_taps, up_taps,
    down_weight,
):
    row = lambda v: v.reshape(1, 2048)
    DMA = pltpu.SemaphoreType.DMA
    return pl.pallas_call(
        kernel,
        name="layer",
        out_shape=jax.ShapeDtypeStruct((512, 256), bf16),
        in_specs=[pl.BlockSpec(memory_space=pltpu.HBM)] * 10,
        out_specs=pl.BlockSpec(memory_space=pltpu.VMEM),
        scratch_shapes=[
            pltpu.VMEM((2, 16, 1408, 128), bf16),
            pltpu.VMEM((2, 16, 704, 128), bf16),
            pltpu.VMEM((8, 16, 64, 128), bf16),
            pltpu.VMEM((4, 2, TOK, 256), bf16),
            pltpu.VMEM((TOK, 256), bf16),
            pltpu.VMEM((4, 32, 64), bf16),
            pltpu.VMEM((3, 1, 2048), f32),
            pltpu.VMEM((2, 3, 1408), f32),
            pltpu.VMEM((2, 2, 3, 704), f32),
            pltpu.VMEM((512, 512), bf16),
            pltpu.VMEM((512, 512), bf16),
            pltpu.VMEM((4, LEN, LEN), bf16),
            pltpu.VMEM((4, 8, 512), f32),
            pltpu.VMEM((4, TOK, 512), bf16),
            pltpu.VMEM((4, 512, 512), bf16),
            pltpu.VMEM((16, TOK, 128), bf16),
            pltpu.VMEM((TOK, 128), f32),
            pltpu.VMEM((2, TOK, 704), bf16),
            pltpu.VMEM((8, TOK, 256), bf16),
            pltpu.VMEM((3, 2, TOK, 256), bf16),
            pltpu.VMEM((2, 2, TOK, 704), f32),
            pltpu.VMEM((2, TOK, 256), bf16),
            DMA((11,)),
            DMA((16,)),
            DMA((16,)),
            DMA((1,)),
            DMA((16,)),
            DMA((16,)),
            DMA((4,)),
            DMA((4,)),
            DMA((2, 3)),
            DMA((1,)),
            DMA((3, 2)),
            DMA((10,)),
            DMA((2,)),
        ],
        compiler_params=pltpu.CompilerParams(
            collective_id=0, has_side_effects=True, vmem_limit_bytes=60 * 1024 * 1024
        ),
    )(
        stream, row(gain_mix), pool_weight, row(pool_gain), row(gain_ffn), gate_weight.T, up_weight.T,
        gate_taps, up_taps, down_weight,
    )


def solution(mesh):
    return jax.shard_map(
        body,
        mesh=mesh,
        in_specs=(
            P("fs", "tp"), P(), P(None, "fs", "tp"), P(), P(), P("fs", "tp"), P("fs", "tp"), P(), P(),
            P("tp", "fs"),
        ),
        out_specs=P("fs", "tp"),
        check_vma=False,
    )
```

time: 96.1 us -> 73.3 us (0.76)
  Pallas kernels: 90.8 us -> 71.5 us
  local copies, waits for them, and re-layouts: 4.27 us -> 1.67 us
    pallas_call x1, Pallas kernels: 90.8 us -> 71.5 us  [body(): pl.pallas_call(kernel, name='layer', out_shape=jax.ShapeDtypeStruct((512,...]
    unnamed x5 -> x1, local copies, waits for them, and re-layouts: 4.27 us -> 1.67 us
where the time goes in v2:
time: 73.3 us; the launch traced here: 73.1 us
  Pallas kernels  71.5 us (98%)
  local copies, waits for them, and re-layouts  1.67 us (2%)
    pallas_call x1, Pallas kernels, body(): pl.pallas_call(kernel, name='layer', out_shape=jax.ShapeDtypeStruct((512,...  71.5 us
    unnamed x1, local copies, waits for them, and re-layouts  1.67 us

profile of v2, /device:TPU:33, one launch (start us, length us, event | category | flops | bytes accessed | tf_op | source)
XLA Modules:
  0.0 73.1 jit_solution(7612232782273625829)
XLA Ops:
  0.0 71.5 %layer.1 = bf16[512,256]{1,0:T(8,128)(2,1)} custom-call(bf16[512,256]{1,0:T(8,128)(2,1)} %stream.1, f32[1,2048]{1,0:T(1,128)} %bitcast.7, bf16[4,32,64]{2,1,0:T(8,128)(2,1)} %pool_weight.1, f32[1,2048]{1,0:T(1,128)} %bitcast.8, f32[1,2048]{1,0:T(1,128)} %bitcast.9, bf16[704,128]{1,0:T(8,128)(2,1)} %bitcast.5, bf16[704,128]{1,0:T(8,128)(2,1)} %bitcast.6, ...), custom_call_target="tpu_custom_call" | custom-call | tf_op jit(solution)/shard_map/layer/pallas_call | solution.py:473
  71.5 1.7 %copy.12 = bf16[512,256]{1,0:T(8,128)(2,1)} copy(bf16[512,256]{1,0:T(8,128)(2,1)} %layer.1) | data formatting | bytes 524288

commit v3 on v2

--- a/solution.py
+++ b/solution.py
@@ -25,7 +25,7 @@
     down_weight,
     out,
     gu, dn, pw, xs, sv, pv, gv, tv, taps, perm, unperm, band, gains, xg, wg, nf, acc, hid,
-    pb, rbuf, sums, relay_in,
+    pb, rbuf, sums, relay_in, early,
     lsem, gsem, dsem, psem, gd, dd, pys, pds, xys, xds, rsem, ssem, relsem,
 ):
     fs, tp = lax.axis_index("fs"), lax.axis_index("tp")
@@ -41,8 +41,8 @@
     partner = (fs, y * 2 + (1 - c))
 
     barrier = pltpu.get_barrier_semaphore()
-    others = [(dx, dz) for dz in (0, 1, -1, 2) for dx in (0, 1, -1, 2)][1:]
-    peers = [(at_fs(dx, dz), tp) for dx, dz in others]
+    near = [(dx, dz) for dz in (0, 1, -1) for dx in (0, 1, -1)][1:]
+    peers = [(at_fs(dx, dz), tp) for dx, dz in near]
     peers += [(fs, at_y(dy, core)) for dy in (1, -1) for core in (0, 1)] + [partner]
     for peer in peers:
         pl.semaphore_signal(barrier, inc=1, device_id=peer, device_id_type=MESH)
@@ -149,7 +149,7 @@
     RIGHT, LEFT, UP, DOWN = (1, 0), (-1, 0), (0, 1), (0, -1)
     remote(sv, xs.at[y, c], ssem.at[4], xds.at[0], partner).start()
     piece_out(c)
-    for dx, dz in others:
+    for dx, dz in near:
         mine = pw.at[tp, fs]
         remote(mine, mine, ssem.at[0], psem.at[0], (at_fs(dx, dz), tp)).start()
     gup.run((0, 0, False, [RIGHT]))
@@ -183,26 +183,47 @@
         taps[core, 0] = tv[0, :, a : a + 704]
         taps[core, 1] = tv[1, :, a : a + 704]
 
+    got(pw.at[tp, 0:8], psem.at[0])
+
+    def onward(ox, oz, half, dx, dz):
+        ref = pw.at[tp, at_fs(ox, oz), pl.ds(32 * half, 32)]
+        remote(ref, ref, ssem.at[0], psem.at[1], (at_fs(dx, dz), tp)).start()
+
+    for o in (0, 1, -1):
+        onward(-1, o, 0, 1, 0)
+        onward(1, o, 1, -1, 0)
+        onward(o, -1, 0, 0, 1)
+        onward(o, 1, 1, 0, -1)
+    onward(-1, -1, 0, 1, 1)
+    onward(1, 1, 1, -1, -1)
     gup.run((1, 0, True, [RIGHT]))
     gup.run((0, 0, False, [DOWN]))
     gup.run((1, 0, False, [UP]))
-    got(pw.at[tp, 0:15], psem.at[0])
-
-    def columns(dy, core):
-        return pw.at[at_y(dy, core)]
-
-    def pool_across(i, dy):
-        remote(columns(dy, c), columns(dy, c), ssem.at[7], pds.at[i], partner).start()
-
-    remote(columns(0, c), columns(0, c), ssem.at[8], pys.at[0], (fs, at_y(1, c))).start()
-    remote(columns(0, c), columns(0, c), ssem.at[8], pys.at[1], (fs, at_y(-1, c))).start()
-    pool_across(0, 0)
-    gup.run((2, 0, True, [UP]))
-
     got(piece(-1, 0), xys.at[0, 0])
     remote(piece(-1, 0), piece(-1, 0), ssem.at[3], xys.at[0, 2], (fs, at_y(1, c))).start()
     got(piece(1, 1), xys.at[1, 1])
     remote(piece(1, 1), piece(1, 1), ssem.at[3], xys.at[1, 2], (fs, at_y(-1, c))).start()
+    got(pw.at[tp, 0:7], psem.at[1])
+
+    def columns(dy, core):
+        return pw.at[at_y(dy, core)]
+
+    def pool_across(i, dy):
+        remote(columns(dy, c), columns(dy, c), ssem.at[7], pds.at[i], partner).start()
+
+    def half_out(dy, half, sem, to):
+        ref = columns(dy, c).at[pl.ds(8 * half, 8)]
+        remote(ref, ref, ssem.at[8], pys.at[sem], (fs, at_y(to, c))).start()
+
+    def half_in(dy, half, sem):
+        got(columns(dy, c).at[pl.ds(8 * half, 8)], pys.at[sem])
+
+    half_out(0, 0, 0, 1)
+    half_out(0, 1, 2, -1)
+    half_out(0, 1, 1, 1)
+    half_out(0, 0, 3, -1)
+    pool_across(0, 0)
+    gup.run((2, 0, True, [UP]))
     gup.run((-1, 0, True, [UP]))
     gup.run((0, 1, True, [UP]), (1, 0, False, [DOWN]), (2, 0, False, [DOWN]), (-1, 0, False, [DOWN]))
 
@@ -231,41 +252,41 @@
     got(piece(1, 0), xys.at[0, 1])
     got(piece(-1, 1), xys.at[1, 0])
     regroup(y, 0)
+    regroup((y + 1) % 4, 0)
+    regroup((y + 3) % 4, 0)
     gup.run((0, -1, True, []))
     across(gu, gd, ssem.at[5], NEAR)
-    regroup((y + 1) % 4, 0)
-    regroup((y + 3) % 4, 0)
+    gup.run((1, 1, True, [UP]))
+    down.run((0, 0, False, [RIGHT]))
     got(columns(0, 1 - c), pds.at[0])
     unpack(y, 0)
-    got(columns(-1, c), pys.at[0])
-    half = columns(-1, c).at[0:8]
-    remote(half, half, ssem.at[8], pys.at[2], (fs, at_y(1, c))).start()
-    pool_across(1, -1)
-    got(columns(1, c), pys.at[1])
-    half = columns(1, c).at[8:16]
-    remote(half, half, ssem.at[8], pys.at[3], (fs, at_y(-1, c))).start()
-    pool_across(2, 1)
-    gup.run((1, 1, True, [UP]))
-    down.run((0, 0, False, [RIGHT]))
+    half_in(-1, 0, 0)
+    half_out(-1, 0, 4, 1)
+    half_in(1, 1, 2)
+    half_out(1, 1, 5, -1)
     gup.run((2, 1, True, [UP]))
-    down.run((0, 0, False, [UP]))
-    gup.run((-1, 1, True, [UP]))
-    down.run((0, 0, False, [LEFT]))
-    down.run((0, 0, False, [DOWN]))
     got(piece(2, 0), xys.at[0, 2])
     got(piece(2, 1), xys.at[1, 2])
     regroup((y + 2) % 4, 0)
+    gup.run((-1, 1, True, [UP]))
+    down.run((0, 0, False, [UP]))
+    down.run((0, 0, False, [LEFT]))
+    down.run((0, 0, False, [DOWN]))
+    half_in(-1, 1, 1)
+    pool_across(1, -1)
+    half_in(1, 0, 3)
+    pool_across(2, 1)
     got(columns(-1, 1 - c), pds.at[1])
     unpack((y + 3) % 4, 0)
     got(columns(1, 1 - c), pds.at[2])
     unpack((y + 1) % 4, 0)
-    got(columns(2, c).at[0:8], pys.at[2])
-    got(columns(2, c).at[8:16], pys.at[3])
+    half_in(2, 0, 4)
+    half_in(2, 1, 5)
     pool_across(3, 2)
+    gup.run((0, 2, True, []))
+    across(gu, gd, ssem.at[5], FAR)
     got(columns(2, 1 - c), pds.at[3])
     unpack((y + 2) % 4, 0)
-    gup.run((0, 2, True, []))
-    across(gu, gd, ssem.at[5], FAR)
 
     scale = lax.rsqrt(jnp.sum(acc[...], axis=1, keepdims=True) * (1.0 / 2048) + EPS)
     acc[...] = jnp.zeros_like(acc)
@@ -345,117 +366,144 @@
     gup.run((1, -1, True, []), (-1, -1, True, []), (2, -1, True, []))
     across(gu, gd, ssem.at[5], DIAG)
     gather_up(c, 1)
+    down.run((1, 0, True, [RIGHT, UP]))
     across_wait(gu, gd, SETS[1])
     gather_up(1 - c, 1)
-    down.run((1, 0, True, [RIGHT, UP]))
-    gup.run((1, 2, True, []), (2, 2, True, []))
+    gup.run((1, 2, True, []), (2, 2, True, []), (-1, 2, True, []))
+    across(gu, gd, ssem.at[5], KNIGHT + [(2, 2)])
     down.run((0, 1, True, [UP]))
-    gup.run((-1, 2, True, []))
-    across(gu, gd, ssem.at[5], KNIGHT + [(2, 2)])
     units(c, 0)
-    down.run((-1, 0, True, [UP, DOWN]), (1, 0, False, [DOWN]))
     units(c, 1)
+    down.run((-1, 0, True, [UP, DOWN]))
+    across_wait(gu, gd, SETS[2])
+    units(c, 2)
     down.run((0, -1, True, []))
     across(dn, dd, ssem.at[6], NEAR)
-    units(c, 2)
-    down.run((2, 0, True, [UP, DOWN]))
-    across_wait(gu, gd, SETS[2])
     units(1 - c, 0)
+    down.run((2, 0, True, [UP]))
+    down.run((1, 0, False, [DOWN]), (2, 0, False, [DOWN]))
+    units(1 - c, 1)
     down.run((1, 1, True, [UP]))
-    units(1 - c, 1)
+    down.run((0, 2, True, []))
+    across(dn, dd, ssem.at[6], FAR)
+    units(1 - c, 2)
     down.run((-1, 1, True, [UP]))
-    units(1 - c, 2)
-
-    way = {(0, 0): 1, (0, 1): -1, (1, 0): -1, (1, 1): 1, (-1, 0): 1, (-1, 1): -1, (2, 0): 1, (2, 1): -1}
 
     def pair_of(dz, other):
         cols = x // 2 if other == 0 else 1 - x // 2
         zk = (z + dz + 4) % 4
         return zk * 2 + cols, cols, (zk - y + 4) % 4
 
-    def to_owner(k, dy, cols):
-        slot = 1 if dy == 1 else 2
-        device = (fs, at_y(dy, cols))
-        remote(pb.at[k], rbuf.at[slot, c], ssem.at[9], rsem.at[slot, c], device).start()
+    def to_owner(k, h, dy, cols):
+        slot, device = (3 - dy) // 2, (fs, at_y(dy, cols))
+        remote(pb.at[k, h], rbuf.at[slot, c, h], ssem.at[9], rsem.at[slot, c, h], device).start()
+
+    def hand_on(k, h, cols, role):
+        dy = 1 - 2 * h
+
+        @pl.when(role == 2)
+        def _():
+            there, device = relay_in.at[h, cols], (fs, at_y(dy, c))
+            remote(pb.at[k, h], there, ssem.at[9], relsem.at[h, cols], device).start()
+
+        @pl.when(role == 3 - 2 * h)
+        def _():
+            to_owner(k, h, -dy, cols)
+
+        @pl.when((role == 0) & (cols == c))
+        def _():
+            rbuf[0, c, h] = pb[k, h]
+
+        @pl.when((role == 0) & (cols != c))
+        def _():
+            remote(pb.at[k, h], rbuf.at[0, c, h], ssem.at[9], rsem.at[0, c, h], partner).start()
+
+    def part_of(core, k):
+        block = concat([dn[core, 2 * k], dn[core, 2 * k + 1]], 1)
+        return jnp.dot(hid[core], block, preferred_element_type=f32)
+
+    def own_part(dz, other, at):
+        k, cols, role = pair_of(dz, other)
+        early[at] = part_of(c, k)
+
+    def columns_done(k, cols, role, total):
+        for h in range(2):
+            pb[k, h] = total[:, 128 * h : 128 * h + 128].astype(bf16)
+        for h in range(2):
+            hand_on(k, h, cols, role)
 
     def owner_columns(dz, other):
         k, cols, role = pair_of(dz, other)
-        dy = way[dz, other]
+        columns_done(k, cols, role, part_of(c, k) + part_of(1 - c, k))
+
+    def owner_rest(dz, other, at):
+        k, cols, role = pair_of(dz, other)
+        columns_done(k, cols, role, early[at] + part_of(1 - c, k))
+
+    def owner_half(dz, other, h):
+        k, cols, role = pair_of(dz, other)
         total = None
         for core in range(2):
-            block = concat([dn[core, 2 * k], dn[core, 2 * k + 1]], 1)
-            part = jnp.dot(hid[core], block, preferred_element_type=f32)
+            part = jnp.dot(hid[core], dn[core, 2 * k + h], preferred_element_type=f32)
             total = part if total is None else total + part
-        pb[k] = total.astype(bf16)
-
-        @pl.when((role == 0) & (cols == c))
-        def _():
-            rbuf[0, c] = pb[k]
-
-        @pl.when((role == 0) & (cols != c))
-        def _():
-            remote(pb.at[k], rbuf.at[0, c], ssem.at[9], rsem.at[0, c], partner).start()
-
-        @pl.when(role == (3 if dy == 1 else 1))
-        def _():
-            to_owner(k, -dy, cols)
-
-        @pl.when(role == 2)
-        def _():
-            slot = (1 - dy) // 2
-            device = (fs, at_y(dy, c))
-            remote(pb.at[k], relay_in.at[slot], ssem.at[9], relsem.at[slot], device).start()
+        pb[k, h] = total.astype(bf16)
+        hand_on(k, h, cols, role)
 
     def owner_added(dz, other):
         k, cols, role = pair_of(dz, other)
-        dy = way[dz, other]
-        slot = (1 - dy) // 2
-
-        @pl.when(role == (1 if dy == 1 else 3))
-        def _():
-            got(relay_in.at[slot], relsem.at[slot])
-            pb[k] = (pb[k].astype(f32) + relay_in[slot].astype(f32)).astype(bf16)
-            to_owner(k, dy, cols)
+        for h in range(2):
+
+            @pl.when(role == 1 + 2 * h)
+            def _():
+                got(relay_in.at[h, cols], relsem.at[h, cols])
+                pb[k, h] = (pb[k, h].astype(f32) + relay_in[h, cols].astype(f32)).astype(bf16)
+                to_owner(k, h, 1 - 2 * h, cols)
 
     across_wait(dn, dd, [(0, 0)] + NEAR)
     owner_columns(0, 0)
-    down.run((0, 2, True, []))
-    across(dn, dd, ssem.at[6], FAR)
-    down.run((1, -1, True, []), (-1, -1, True, []), (2, -1, True, []))
-    across(dn, dd, ssem.at[6], DIAG)
     across_wait(dn, dd, FAR)
     owner_columns(0, 1)
     down.run((2, 1, True, [UP]))
+    down.run((1, -1, True, []), (-1, -1, True, []))
+    across(dn, dd, ssem.at[6], DIAG)
+    own_part(1, 0, 0)
+    own_part(-1, 0, 1)
     owner_added(0, 0)
-    down.run((1, 2, True, []), (-1, 2, True, []))
+    across_wait(dn, dd, DIAG)
+    owner_rest(1, 0, 0)
+    owner_rest(-1, 0, 1)
+    owner_added(0, 1)
+    down.run((2, -1, True, []), (1, 2, True, []), (-1, 2, True, []))
     across(dn, dd, ssem.at[6], KNIGHT)
-    across_wait(dn, dd, DIAG)
-    owner_columns(1, 0)
-    owner_columns(-1, 0)
+    own_part(2, 0, 0)
+    own_part(1, 1, 1)
+    own_part(-1, 1, 2)
+    across_wait(dn, dd, KNIGHT)
+    owner_rest(2, 0, 0)
     down.run((2, 2, True, []))
     across(dn, dd, ssem.at[6], [(2, 2)])
-    across_wait(dn, dd, KNIGHT)
-    owner_columns(2, 0)
-    owner_columns(1, 1)
-    owner_added(0, 1)
-    owner_columns(-1, 1)
+    owner_half(2, 1, 1 - x % 2)
+    owner_rest(1, 1, 1)
+    owner_rest(-1, 1, 2)
+    across_wait(dn, dd, [(2, 2)])
+    owner_half(2, 1, x % 2)
     owner_added(1, 0)
-    across_wait(dn, dd, [(2, 2)])
-    owner_columns(2, 1)
     owner_added(-1, 0)
     owner_added(2, 0)
     owner_added(1, 1)
     owner_added(-1, 1)
     owner_added(2, 1)
 
-    got(rbuf.at[1, 0], rsem.at[1, 0])
-    got(rbuf.at[1, 1], rsem.at[1, 1])
-    got(rbuf.at[2, 0], rsem.at[2, 0])
-    got(rbuf.at[2, 1], rsem.at[2, 1])
-    got(rbuf.at[0, 1 - c], rsem.at[0, 1 - c])
+    for slot in (1, 2):
+        for core in range(2):
+            for h in range(2):
+                got(rbuf.at[slot, core, h], rsem.at[slot, core, h])
+    for h in range(2):
+        got(rbuf.at[0, 1 - c, h], rsem.at[0, 1 - c, h])
     for core in range(2):
-        total = rbuf[0, core].astype(f32) + rbuf[1, core].astype(f32) + rbuf[2, core].astype(f32)
-        out[TOK * core : TOK * core + TOK, :] = total.astype(bf16)
+        for h in range(2):
+            total = sum(rbuf[slot, core, h].astype(f32) for slot in range(3))
+            out[TOK * core : TOK * core + TOK, 128 * h : 128 * h + 128] = total.astype(bf16)
 
     for ref, i in (
         (pw.at[0, 0:15], 0), (gu.at[0, 0:15], 1), (dn.at[0, 0:15], 2), (xs.at[0:3], 3), (sv, 4),
@@ -495,23 +543,24 @@
             pltpu.VMEM((16, TOK, 128), bf16),
             pltpu.VMEM((TOK, 128), f32),
             pltpu.VMEM((2, TOK, 704), bf16),
-            pltpu.VMEM((8, TOK, 256), bf16),
-            pltpu.VMEM((3, 2, TOK, 256), bf16),
+            pltpu.VMEM((8, 2, TOK, 128), bf16),
+            pltpu.VMEM((3, 2, 2, TOK, 128), bf16),
             pltpu.VMEM((2, 2, TOK, 704), f32),
-            pltpu.VMEM((2, TOK, 256), bf16),
+            pltpu.VMEM((2, 2, TOK, 128), bf16),
+            pltpu.VMEM((3, TOK, 256), f32),
             DMA((11,)),
             DMA((16,)),
             DMA((16,)),
-            DMA((1,)),
+            DMA((2,)),
             DMA((16,)),
             DMA((16,)),
-            DMA((4,)),
+            DMA((6,)),
             DMA((4,)),
             DMA((2, 3)),
             DMA((1,)),
-            DMA((3, 2)),
+            DMA((3, 2, 2)),
             DMA((10,)),
-            DMA((2,)),
+            DMA((2, 2)),
         ],
         compiler_params=pltpu.CompilerParams(
             collective_id=0, has_side_effects=True, vmem_limit_bytes=60 * 1024 * 1024

time: 73.3 us -> 69.5 us (0.948)
  Pallas kernels: 71.5 us -> 67.5 us
    pallas_call x1, Pallas kernels: 71.5 us -> 67.5 us  [body(): pl.pallas_call(kernel, name='layer', out_shape=jax.ShapeDtypeStruct((512,...]
where the time goes in v3:
time: 69.5 us; the launch traced here: 69.2 us
  Pallas kernels  67.5 us (97%)
  local copies, waits for them, and re-layouts  1.67 us (2%)
    pallas_call x1, Pallas kernels, body(): pl.pallas_call(kernel, name='layer', out_shape=jax.ShapeDtypeStruct((512,...  67.5 us
    unnamed x1, local copies, waits for them, and re-layouts  1.67 us

profile of v3, /device:TPU:33, one launch (start us, length us, event | category | flops | bytes accessed | tf_op | source)
XLA Modules:
  0.0 69.2 jit_solution(18434922948688430183)
XLA Ops:
  0.0 67.5 %layer.1 = bf16[512,256]{1,0:T(8,128)(2,1)} custom-call(bf16[512,256]{1,0:T(8,128)(2,1)} %stream.1, f32[1,2048]{1,0:T(1,128)} %bitcast.7, bf16[4,32,64]{2,1,0:T(8,128)(2,1)} %pool_weight.1, f32[1,2048]{1,0:T(1,128)} %bitcast.8, f32[1,2048]{1,0:T(1,128)} %bitcast.9, bf16[704,128]{1,0:T(8,128)(2,1)} %bitcast.5, bf16[704,128]{1,0:T(8,128)(2,1)} %bitcast.6, ...), custom_call_target="tpu_custom_call" | custom-call | tf_op jit(solution)/shard_map/layer/pallas_call | solution.py:521
  67.5 1.7 %copy.12 = bf16[512,256]{1,0:T(8,128)(2,1)} copy(bf16[512,256]{1,0:T(8,128)(2,1)} %layer.1) | data formatting | bytes 524288

commit v4 on v3

--- a/solution.py
+++ b/solution.py
@@ -77,8 +77,9 @@
         )
 
     class Tree:
-        def __init__(self, block, rows, recv, send):
+        def __init__(self, block, rows, recv, send, cross, cross_send):
             self.block, self.rows, self.recv, self.send = block, rows, recv, send
+            self.cross, self.cross_send = cross, cross_send
 
         def ref(self, q, a, b):
             color, sign = q // 2, 1 - 2 * (q % 2)
@@ -112,23 +113,23 @@
                 def f(q):
                     for da, db in steps:
                         self.push(q, a, b, da, db)
-
-                if steps:
-                    self.each(f)
-
-    gup = Tree(lambda j: gu.at[c, j], 352, gsem, ssem.at[1])
-    down = Tree(lambda j: dn.at[c, j], 176, dsem, ssem.at[2])
-
-    def across(blocks, recv, send, offsets):
-        for dx, dz in offsets:
-            j, pos = at_fs(dx, dz), (dx % 4) * 4 + dz % 4
-            remote(blocks.at[c, j], blocks.at[c, j], send, recv.at[pos], partner).start()
-
-    def across_wait(blocks, recv, offsets):
-        for dx, dz in offsets:
-            j, pos = at_fs(dx, dz), (dx % 4) * 4 + dz % 4
-            ref = blocks.at[1 - c, j]
-            pltpu.make_async_copy(ref, ref, recv.at[pos]).wait()
+                    if wait:
+                        ref = self.ref(q, a, b)
+                        pos = (a % 4) * 4 + b % 4
+                        remote(ref, ref, self.cross_send, self.cross.at[pos], partner).start()
+
+                self.each(f)
+
+    gup = Tree(lambda j: gu.at[c, j], 352, gsem, ssem.at[1], gd, ssem.at[5])
+    down = Tree(lambda j: dn.at[c, j], 176, dsem, ssem.at[2], dd, ssem.at[6])
+
+    def across(blocks, recv, send):
+        remote(blocks.at[c, fs], blocks.at[c, fs], send, recv.at[0], partner).start()
+
+    def across_wait(blocks, recv, steps):
+        for a, b in steps:
+            ref = blocks.at[1 - c, fs]
+            pltpu.make_async_copy(ref, ref, recv.at[(a % 4) * 4 + b % 4]).wait()
 
     NEAR = [(1, 0), (-1, 0), (0, 1), (0, -1)]
     FAR = [(2, 0), (0, 2)]
@@ -155,8 +156,8 @@
     gup.run((0, 0, False, [RIGHT]))
     gup.run((0, 0, False, [UP]))
     gup.run((0, 0, False, [LEFT]))
-    across(gu, gd, ssem.at[5], [(0, 0)])
-    across(dn, dd, ssem.at[6], [(0, 0)])
+    across(gu, gd, ssem.at[5])
+    across(dn, dd, ssem.at[6])
 
     d, n = iota((512, 512), 0), iota((512, 512), 1)
     perm[...] = ((d % 4) * 128 + d // 4 == n).astype(bf16)
@@ -255,7 +256,6 @@
     regroup((y + 1) % 4, 0)
     regroup((y + 3) % 4, 0)
     gup.run((0, -1, True, []))
-    across(gu, gd, ssem.at[5], NEAR)
     gup.run((1, 1, True, [UP]))
     down.run((0, 0, False, [RIGHT]))
     got(columns(0, 1 - c), pds.at[0])
@@ -284,7 +284,6 @@
     half_in(2, 1, 5)
     pool_across(3, 2)
     gup.run((0, 2, True, []))
-    across(gu, gd, ssem.at[5], FAR)
     got(columns(2, 1 - c), pds.at[3])
     unpack((y + 2) % 4, 0)
 
@@ -364,13 +363,11 @@
     across_wait(gu, gd, SETS[0])
     gather_up(1 - c, 0)
     gup.run((1, -1, True, []), (-1, -1, True, []), (2, -1, True, []))
-    across(gu, gd, ssem.at[5], DIAG)
     gather_up(c, 1)
     down.run((1, 0, True, [RIGHT, UP]))
     across_wait(gu, gd, SETS[1])
     gather_up(1 - c, 1)
     gup.run((1, 2, True, []), (2, 2, True, []), (-1, 2, True, []))
-    across(gu, gd, ssem.at[5], KNIGHT + [(2, 2)])
     down.run((0, 1, True, [UP]))
     units(c, 0)
     units(c, 1)
@@ -378,14 +375,12 @@
     across_wait(gu, gd, SETS[2])
     units(c, 2)
     down.run((0, -1, True, []))
-    across(dn, dd, ssem.at[6], NEAR)
     units(1 - c, 0)
     down.run((2, 0, True, [UP]))
     down.run((1, 0, False, [DOWN]), (2, 0, False, [DOWN]))
     units(1 - c, 1)
     down.run((1, 1, True, [UP]))
     down.run((0, 2, True, []))
-    across(dn, dd, ssem.at[6], FAR)
     units(1 - c, 2)
     down.run((-1, 1, True, [UP]))
 
@@ -439,15 +434,6 @@
     def owner_rest(dz, other, at):
         k, cols, role = pair_of(dz, other)
         columns_done(k, cols, role, early[at] + part_of(1 - c, k))
-
-    def owner_half(dz, other, h):
-        k, cols, role = pair_of(dz, other)
-        total = None
-        for core in range(2):
-            part = jnp.dot(hid[core], dn[core, 2 * k + h], preferred_element_type=f32)
-            total = part if total is None else total + part
-        pb[k, h] = total.astype(bf16)
-        hand_on(k, h, cols, role)
 
     def owner_added(dz, other):
         k, cols, role = pair_of(dz, other)
@@ -465,7 +451,6 @@
     owner_columns(0, 1)
     down.run((2, 1, True, [UP]))
     down.run((1, -1, True, []), (-1, -1, True, []))
-    across(dn, dd, ssem.at[6], DIAG)
     own_part(1, 0, 0)
     own_part(-1, 0, 1)
     owner_added(0, 0)
@@ -474,19 +459,17 @@
     owner_rest(-1, 0, 1)
     owner_added(0, 1)
     down.run((2, -1, True, []), (1, 2, True, []), (-1, 2, True, []))
-    across(dn, dd, ssem.at[6], KNIGHT)
     own_part(2, 0, 0)
     own_part(1, 1, 1)
     own_part(-1, 1, 2)
     across_wait(dn, dd, KNIGHT)
     owner_rest(2, 0, 0)
     down.run((2, 2, True, []))
-    across(dn, dd, ssem.at[6], [(2, 2)])
-    owner_half(2, 1, 1 - x % 2)
     owner_rest(1, 1, 1)
     owner_rest(-1, 1, 2)
+    own_part(2, 1, 0)
     across_wait(dn, dd, [(2, 2)])
-    owner_half(2, 1, x % 2)
+    owner_rest(2, 1, 0)
     owner_added(1, 0)
     owner_added(-1, 0)
     owner_added(2, 0)
@@ -563,11 +546,12 @@
             DMA((2, 2)),
         ],
         compiler_params=pltpu.CompilerParams(
-            collective_id=0, has_side_effects=True, vmem_limit_bytes=60 * 1024 * 1024
+            collective_id=0, has_side_effects=True, vmem_limit_bytes=50 * 1024 * 1024
         ),
     )(
+        *[pltpu.with_memory_space_constraint(v, pltpu.HBM) for v in (
         stream, row(gain_mix), pool_weight, row(pool_gain), row(gain_ffn), gate_weight.T, up_weight.T,
-        gate_taps, up_taps, down_weight,
+        gate_taps, up_taps, down_weight)]
     )
 
 

time: 69.5 us -> 66.9 us (0.963)
  Pallas kernels: 67.5 us -> 65.4 us
  local copies, waits for them, and re-layouts: 1.67 us -> 0.71 us
    pallas_call x1, Pallas kernels: 67.5 us -> 65.4 us  [body(): pl.pallas_call(kernel, name='layer', out_shape=jax.ShapeDtypeStruct((512,...]
    unnamed x1, local copies, waits for them, and re-layouts: 1.67 us -> 0.71 us
where the time goes in v4:
time: 66.9 us; the launch traced here: 66.1 us
  Pallas kernels  65.4 us (98%)
  local copies, waits for them, and re-layouts  0.71 us (1%)
    pallas_call x1, Pallas kernels, body(): pl.pallas_call(kernel, name='layer', out_shape=jax.ShapeDtypeStruct((512,...  65.4 us

profile of v4, /device:TPU:33, one launch (start us, length us, event | category | flops | bytes accessed | tf_op | source)
XLA Modules:
  0.0 66.1 jit_solution(11981413357057496326)
XLA Ops:
  0.0 65.4 %layer.1 = bf16[512,256]{1,0:T(8,128)(2,1)S(1)} custom-call(bf16[512,256]{1,0:T(8,128)(2,1)} %stream.1, f32[1,2048]{1,0:T(1,128)} %bitcast.7, bf16[4,32,64]{2,1,0:T(8,128)(2,1)} %pool_weight.1, f32[1,2048]{1,0:T(1,128)} %bitcast.8, f32[1,2048]{1,0:T(1,128)} %bitcast.9, bf16[704,128]{1,0:T(8,128)(2,1)} %bitcast.5, bf16[704,128]{1,0:T(8,128)(2,1)} %bitcast.6, ...), custom_call_target="tpu_custom_call" | custom-call | tf_op jit(solution)/shard_map/layer/pallas_call | solution.py:504
  65.4 0.7 %copy.12 = bf16[512,256]{1,0:T(8,128)(2,1)} copy(bf16[512,256]{1,0:T(8,128)(2,1)S(1)} %layer.1) | data formatting | bytes 524288

commit v5 on v4

--- a/solution.py
+++ b/solution.py
@@ -9,6 +9,7 @@
 bf16, f32 = jnp.bfloat16, jnp.float32
 EPS = 1e-6
 LEN = 128
+PIECES = (0, 1)
 TOK = 256
 
 
@@ -51,9 +52,9 @@
         (pool_weight, pv),
         (gate_weight, gu.at[c, fs, pl.ds(0, 704)]),
         (up_weight, gu.at[c, fs, pl.ds(704, 704)]),
-        (down_weight, dn.at[c, fs]),
         (stream.at[pl.ds(pl.multiple_of(c * TOK, TOK), TOK)], xs.at[y, c]),
         (stream.at[pl.ds(pl.multiple_of((1 - c) * TOK, TOK), TOK)], sv),
+        (down_weight, dn.at[c, fs]),
         (gain_mix, gv.at[0]),
         (pool_gain, gv.at[1]),
         (gain_ffn, gv.at[2]),
@@ -66,7 +67,7 @@
     loads[0].wait()
     for p in range(2):
         pw[tp, fs, 32 * p : 32 * p + 32, :] = concat([pv[2 * p], pv[2 * p + 1]], 1)
-    for load in loads[1:]:
+    for load in loads[1:5]:
         load.wait()
     pl.semaphore_wait(barrier, len(peers))
 
@@ -75,6 +76,12 @@
             src_ref=src, dst_ref=dst, send_sem=send, recv_sem=recv, device_id=device,
             device_id_type=MESH,
         )
+
+    def got(ref, sem):
+        pltpu.make_async_copy(ref, ref, sem).wait()
+
+    def group(a, b):
+        return {0: 0, 1: 0, 4: 1, 2: 2, 5: 3, 8: 4}[a * a + b * b]
 
     class Tree:
         def __init__(self, block, rows, recv, send, cross, cross_send):
@@ -115,8 +122,8 @@
                         self.push(q, a, b, da, db)
                     if wait:
                         ref = self.ref(q, a, b)
-                        pos = (a % 4) * 4 + b % 4
-                        remote(ref, ref, self.cross_send, self.cross.at[pos], partner).start()
+                        sem = self.cross.at[group(a, b)]
+                        remote(ref, ref, self.cross_send, sem, partner).start()
 
                 self.each(f)
 
@@ -126,16 +133,14 @@
     def across(blocks, recv, send):
         remote(blocks.at[c, fs], blocks.at[c, fs], send, recv.at[0], partner).start()
 
-    def across_wait(blocks, recv, steps):
-        for a, b in steps:
-            ref = blocks.at[1 - c, fs]
-            pltpu.make_async_copy(ref, ref, recv.at[(a % 4) * 4 + b % 4]).wait()
+    def across_wait(blocks, recv, i):
+        count = (5, 2, 4, 4, 1)[i]
+        got(blocks.at[1 - c, 0:count], recv.at[i])
 
     NEAR = [(1, 0), (-1, 0), (0, 1), (0, -1)]
     FAR = [(2, 0), (0, 2)]
     DIAG = [(1, 1), (1, -1), (-1, 1), (-1, -1)]
     KNIGHT = [(2, 1), (2, -1), (1, 2), (-1, 2)]
-    ALL = [(0, 0)] + NEAR + FAR + DIAG + KNIGHT + [(2, 2)]
 
     def piece(dy, p):
         return xs.at[(y + dy + 4) % 4, p]
@@ -143,9 +148,6 @@
     def piece_out(p):
         remote(piece(0, p), piece(0, p), ssem.at[3], xys.at[p, 0], (fs, at_y(1, c))).start()
         remote(piece(0, p), piece(0, p), ssem.at[3], xys.at[p, 1], (fs, at_y(-1, c))).start()
-
-    def got(ref, sem):
-        pltpu.make_async_copy(ref, ref, sem).wait()
 
     RIGHT, LEFT, UP, DOWN = (1, 0), (-1, 0), (0, 1), (0, -1)
     remote(sv, xs.at[y, c], ssem.at[4], xds.at[0], partner).start()
@@ -157,6 +159,8 @@
     gup.run((0, 0, False, [UP]))
     gup.run((0, 0, False, [LEFT]))
     across(gu, gd, ssem.at[5])
+    for load in loads[5:]:
+        load.wait()
     across(dn, dd, ssem.at[6])
 
     d, n = iota((512, 512), 0), iota((512, 512), 1)
@@ -360,29 +364,29 @@
         hid[core, :, at : at + width] = (a / (1.0 + jnp.exp(-a)) * b).astype(bf16)
 
     gather_up(c, 0)
-    across_wait(gu, gd, SETS[0])
+    across_wait(gu, gd, 0)
     gather_up(1 - c, 0)
     gup.run((1, -1, True, []), (-1, -1, True, []), (2, -1, True, []))
     gather_up(c, 1)
     down.run((1, 0, True, [RIGHT, UP]))
-    across_wait(gu, gd, SETS[1])
+    across_wait(gu, gd, 1)
+    across_wait(gu, gd, 2)
     gather_up(1 - c, 1)
     gup.run((1, 2, True, []), (2, 2, True, []), (-1, 2, True, []))
+    units(c, 0)
     down.run((0, 1, True, [UP]))
-    units(c, 0)
     units(c, 1)
     down.run((-1, 0, True, [UP, DOWN]))
-    across_wait(gu, gd, SETS[2])
     units(c, 2)
+    across_wait(gu, gd, 3)
+    across_wait(gu, gd, 4)
+    units(1 - c, 0)
     down.run((0, -1, True, []))
-    units(1 - c, 0)
+    units(1 - c, 1)
     down.run((2, 0, True, [UP]))
     down.run((1, 0, False, [DOWN]), (2, 0, False, [DOWN]))
-    units(1 - c, 1)
+    units(1 - c, 2)
     down.run((1, 1, True, [UP]))
-    down.run((0, 2, True, []))
-    units(1 - c, 2)
-    down.run((-1, 1, True, [UP]))
 
     def pair_of(dz, other):
         cols = x // 2 if other == 0 else 1 - x // 2
@@ -398,8 +402,9 @@
 
         @pl.when(role == 2)
         def _():
-            there, device = relay_in.at[h, cols], (fs, at_y(dy, c))
-            remote(pb.at[k, h], there, ssem.at[9], relsem.at[h, cols], device).start()
+            for p in PIECES:
+                there, sem = relay_in.at[h, cols, p], relsem.at[h, cols, p]
+                remote(pb.at[k, h, p], there, ssem.at[9], sem, (fs, at_y(dy, c))).start()
 
         @pl.when(role == 3 - 2 * h)
         def _():
@@ -423,7 +428,8 @@
 
     def columns_done(k, cols, role, total):
         for h in range(2):
-            pb[k, h] = total[:, 128 * h : 128 * h + 128].astype(bf16)
+            for p in PIECES:
+                pb[k, h, p] = total[LEN * p : LEN * p + LEN, 128 * h : 128 * h + 128].astype(bf16)
         for h in range(2):
             hand_on(k, h, cols, role)
 
@@ -435,57 +441,99 @@
         k, cols, role = pair_of(dz, other)
         columns_done(k, cols, role, early[at] + part_of(1 - c, k))
 
+    def part_at(core, steps):
+        block = concat([dn[core, at_fs(dx, dz)] for dx, dz in steps], 1)
+        return jnp.dot(hid[core], block, preferred_element_type=f32)
+
+    def halves_done(steps, total):
+        for i, (dx, dz) in enumerate(steps):
+            j = at_fs(dx, dz)
+            k, h = j // 2, j % 2
+            for p in PIECES:
+                part = total[LEN * p : LEN * p + LEN, 128 * i : 128 * i + 128]
+                pb[k, h, p] = part.astype(bf16)
+            hand_on(k, h, k % 2, (k // 2 - y + 4) % 4)
+
+    def owner_halves(steps):
+        halves_done(steps, part_at(c, steps) + part_at(1 - c, steps))
+
+    def own_halves(steps, at):
+        early[at, :, 0 : 128 * len(steps)] = part_at(c, steps)
+
+    def rest_halves(steps, at):
+        halves_done(steps, early[at, :, 0 : 128 * len(steps)] + part_at(1 - c, steps))
+
+    def add_half(k, h):
+        cols, role = k % 2, (k // 2 - y + 4) % 4
+
+        @pl.when(role == 1 + 2 * h)
+        def _():
+            for p in PIECES:
+                got(relay_in.at[h, cols, p], relsem.at[h, cols, p])
+                total = pb[k, h, p].astype(f32) + relay_in[h, cols, p].astype(f32)
+                pb[k, h, p] = total.astype(bf16)
+                dy = 1 - 2 * h
+                there, sem = rbuf.at[(3 - dy) // 2, c, h, p], rsem.at[(3 - dy) // 2, c, h]
+                remote(pb.at[k, h, p], there, ssem.at[9], sem, (fs, at_y(dy, cols))).start()
+
+    def half_added(dx, dz):
+        j = at_fs(dx, dz)
+        add_half(j // 2, j % 2)
+
     def owner_added(dz, other):
         k, cols, role = pair_of(dz, other)
         for h in range(2):
-
-            @pl.when(role == 1 + 2 * h)
-            def _():
-                got(relay_in.at[h, cols], relsem.at[h, cols])
-                pb[k, h] = (pb[k, h].astype(f32) + relay_in[h, cols].astype(f32)).astype(bf16)
-                to_owner(k, h, 1 - 2 * h, cols)
-
-    across_wait(dn, dd, [(0, 0)] + NEAR)
+            add_half(k, h)
+
+    mate = 1 - 2 * (x % 2)
+    across_wait(dn, dd, 0)
     owner_columns(0, 0)
-    across_wait(dn, dd, FAR)
+    down.run((0, 2, True, []))
+    down.run((-1, 1, True, [UP]))
+    across_wait(dn, dd, 1)
     owner_columns(0, 1)
     down.run((2, 1, True, [UP]))
+    owner_halves([(0, 2)])
     down.run((1, -1, True, []), (-1, -1, True, []))
     own_part(1, 0, 0)
     own_part(-1, 0, 1)
+    own_halves([(-mate, 1), (-mate, -1)], 2)
     owner_added(0, 0)
-    across_wait(dn, dd, DIAG)
+    across_wait(dn, dd, 2)
     owner_rest(1, 0, 0)
     owner_rest(-1, 0, 1)
+    rest_halves([(-mate, 1), (-mate, -1)], 2)
+    down.run((2, -1, True, []), (1, 2, True, []), (-1, 2, True, []))
+    own_halves([(mate, 2), (-mate, 2)], 0)
+    own_halves([(2, 1), (2, -1)], 1)
     owner_added(0, 1)
-    down.run((2, -1, True, []), (1, 2, True, []), (-1, 2, True, []))
-    own_part(2, 0, 0)
-    own_part(1, 1, 1)
-    own_part(-1, 1, 2)
-    across_wait(dn, dd, KNIGHT)
-    owner_rest(2, 0, 0)
+    half_added(0, 2)
+    across_wait(dn, dd, 3)
+    rest_halves([(mate, 2), (-mate, 2)], 0)
     down.run((2, 2, True, []))
-    owner_rest(1, 1, 1)
-    owner_rest(-1, 1, 2)
-    own_part(2, 1, 0)
-    across_wait(dn, dd, [(2, 2)])
-    owner_rest(2, 1, 0)
+    rest_halves([(2, 1), (2, -1)], 1)
+    own_halves([(2, 2)], 0)
+    across_wait(dn, dd, 4)
+    rest_halves([(2, 2)], 0)
     owner_added(1, 0)
     owner_added(-1, 0)
-    owner_added(2, 0)
-    owner_added(1, 1)
-    owner_added(-1, 1)
-    owner_added(2, 1)
+    half_added(-mate, 1)
+    half_added(-mate, -1)
+    half_added(mate, 2)
+    half_added(-mate, 2)
+    half_added(2, 1)
+    half_added(2, -1)
+    half_added(2, 2)
 
     for slot in (1, 2):
         for core in range(2):
             for h in range(2):
-                got(rbuf.at[slot, core, h], rsem.at[slot, core, h])
+                    got(rbuf.at[slot, core, h], rsem.at[slot, core, h])
     for h in range(2):
         got(rbuf.at[0, 1 - c, h], rsem.at[0, 1 - c, h])
     for core in range(2):
         for h in range(2):
-            total = sum(rbuf[slot, core, h].astype(f32) for slot in range(3))
+            total = sum(rbuf[slot, core, h].reshape(TOK, 128).astype(f32) for slot in range(3))
             out[TOK * core : TOK * core + TOK, 128 * h : 128 * h + 128] = total.astype(bf16)
 
     for ref, i in (
@@ -526,24 +574,24 @@
             pltpu.VMEM((16, TOK, 128), bf16),
             pltpu.VMEM((TOK, 128), f32),
             pltpu.VMEM((2, TOK, 704), bf16),
-            pltpu.VMEM((8, 2, TOK, 128), bf16),
-            pltpu.VMEM((3, 2, 2, TOK, 128), bf16),
+            pltpu.VMEM((8, 2, 2, LEN, 128), bf16),
+            pltpu.VMEM((3, 2, 2, 2, LEN, 128), bf16),
             pltpu.VMEM((2, 2, TOK, 704), f32),
-            pltpu.VMEM((2, 2, TOK, 128), bf16),
-            pltpu.VMEM((3, TOK, 256), f32),
+            pltpu.VMEM((2, 2, 2, LEN, 128), bf16),
+            pltpu.VMEM((4, TOK, 256), f32),
             DMA((11,)),
             DMA((16,)),
             DMA((16,)),
             DMA((2,)),
-            DMA((16,)),
-            DMA((16,)),
+            DMA((5,)),
+            DMA((5,)),
             DMA((6,)),
             DMA((4,)),
             DMA((2, 3)),
             DMA((1,)),
             DMA((3, 2, 2)),
             DMA((10,)),
-            DMA((2, 2)),
+            DMA((2, 2, 2)),
         ],
         compiler_params=pltpu.CompilerParams(
             collective_id=0, has_side_effects=True, vmem_limit_bytes=50 * 1024 * 1024

time: 66.9 us -> 66.9 us (level); the launches traced: 66.1 us -> 66.8 us
  Pallas kernels: 65.4 us -> 66.1 us
    pallas_call x1, Pallas kernels: 65.4 us -> 66.1 us  [body(): pl.pallas_call(kernel, name='layer', out_shape=jax.ShapeDtypeStruct((512,...]
where the time goes in v5:
time: 66.9 us; the launch traced here: 66.8 us
  Pallas kernels  66.1 us (99%)
  local copies, waits for them, and re-layouts  0.71 us (1%)
    pallas_call x1, Pallas kernels, body(): pl.pallas_call(kernel, name='layer', out_shape=jax.ShapeDtypeStruct((512,...  66.1 us

profile of v5, /device:TPU:33, one launch (start us, length us, event | category | flops | bytes accessed | tf_op | source)
XLA Modules:
  0.0 66.8 jit_solution(18107887988070614452)
XLA Ops:
  0.0 66.1 %layer.1 = bf16[512,256]{1,0:T(8,128)(2,1)S(1)} custom-call(bf16[512,256]{1,0:T(8,128)(2,1)} %stream.1, f32[1,2048]{1,0:T(1,128)} %bitcast.7, bf16[4,32,64]{2,1,0:T(8,128)(2,1)} %pool_weight.1, f32[1,2048]{1,0:T(1,128)} %bitcast.8, f32[1,2048]{1,0:T(1,128)} %bitcast.9, bf16[704,128]{1,0:T(8,128)(2,1)} %bitcast.5, bf16[704,128]{1,0:T(8,128)(2,1)} %bitcast.6, ...), custom_call_target="tpu_custom_call" | custom-call | tf_op jit(solution)/shard_map/layer/pallas_call | solution.py:552
  66.1 0.7 %copy.12 = bf16[512,256]{1,0:T(8,128)(2,1)} copy(bf16[512,256]{1,0:T(8,128)(2,1)S(1)} %layer.1) | data formatting | bytes 524288

commit v6 on v5

--- a/solution.py
+++ b/solution.py
@@ -376,15 +376,14 @@
     units(c, 0)
     down.run((0, 1, True, [UP]))
     units(c, 1)
-    down.run((-1, 0, True, [UP, DOWN]))
+    down.run((-1, 0, True, [UP, DOWN]), (1, 0, False, [DOWN]))
     units(c, 2)
     across_wait(gu, gd, 3)
     across_wait(gu, gd, 4)
     units(1 - c, 0)
     down.run((0, -1, True, []))
     units(1 - c, 1)
-    down.run((2, 0, True, [UP]))
-    down.run((1, 0, False, [DOWN]), (2, 0, False, [DOWN]))
+    down.run((2, 0, True, [UP, DOWN]))
     units(1 - c, 2)
     down.run((1, 1, True, [UP]))
 
@@ -397,7 +396,7 @@
         slot, device = (3 - dy) // 2, (fs, at_y(dy, cols))
         remote(pb.at[k, h], rbuf.at[slot, c, h], ssem.at[9], rsem.at[slot, c, h], device).start()
 
-    def hand_on(k, h, cols, role):
+    def hand_far(k, h, cols, role):
         dy = 1 - 2 * h
 
         @pl.when(role == 2)
@@ -406,6 +405,9 @@
                 there, sem = relay_in.at[h, cols, p], relsem.at[h, cols, p]
                 remote(pb.at[k, h, p], there, ssem.at[9], sem, (fs, at_y(dy, c))).start()
 
+    def hand_near(k, h, cols, role):
+        dy = 1 - 2 * h
+
         @pl.when(role == 3 - 2 * h)
         def _():
             to_owner(k, h, -dy, cols)
@@ -431,7 +433,9 @@
             for p in PIECES:
                 pb[k, h, p] = total[LEN * p : LEN * p + LEN, 128 * h : 128 * h + 128].astype(bf16)
         for h in range(2):
-            hand_on(k, h, cols, role)
+            hand_far(k, h, cols, role)
+        for h in range(2):
+            hand_near(k, h, cols, role)
 
     def owner_columns(dz, other):
         k, cols, role = pair_of(dz, other)
@@ -445,14 +449,22 @@
         block = concat([dn[core, at_fs(dx, dz)] for dx, dz in steps], 1)
         return jnp.dot(hid[core], block, preferred_element_type=f32)
 
-    def halves_done(steps, total):
+    def halves_done(steps, total, near=True):
         for i, (dx, dz) in enumerate(steps):
             j = at_fs(dx, dz)
             k, h = j // 2, j % 2
             for p in PIECES:
                 part = total[LEN * p : LEN * p + LEN, 128 * i : 128 * i + 128]
                 pb[k, h, p] = part.astype(bf16)
-            hand_on(k, h, k % 2, (k // 2 - y + 4) % 4)
+            hand_far(k, h, k % 2, (k // 2 - y + 4) % 4)
+        if near:
+            near_done(steps)
+
+    def near_done(steps):
+        for dx, dz in steps:
+            j = at_fs(dx, dz)
+            k, h = j // 2, j % 2
+            hand_near(k, h, k % 2, (k // 2 - y + 4) % 4)
 
     def owner_halves(steps):
         halves_done(steps, part_at(c, steps) + part_at(1 - c, steps))
@@ -460,8 +472,8 @@
     def own_halves(steps, at):
         early[at, :, 0 : 128 * len(steps)] = part_at(c, steps)
 
-    def rest_halves(steps, at):
-        halves_done(steps, early[at, :, 0 : 128 * len(steps)] + part_at(1 - c, steps))
+    def rest_halves(steps, at, near=True):
+        halves_done(steps, early[at, :, 0 : 128 * len(steps)] + part_at(1 - c, steps), near)
 
     def add_half(k, h):
         cols, role = k % 2, (k // 2 - y + 4) % 4
@@ -492,26 +504,29 @@
     down.run((-1, 1, True, [UP]))
     across_wait(dn, dd, 1)
     owner_columns(0, 1)
-    down.run((2, 1, True, [UP]))
     owner_halves([(0, 2)])
     down.run((1, -1, True, []), (-1, -1, True, []))
     own_part(1, 0, 0)
     own_part(-1, 0, 1)
     own_halves([(-mate, 1), (-mate, -1)], 2)
-    owner_added(0, 0)
     across_wait(dn, dd, 2)
     owner_rest(1, 0, 0)
+    down.run((2, 1, True, [UP]))
     owner_rest(-1, 0, 1)
     rest_halves([(-mate, 1), (-mate, -1)], 2)
-    down.run((2, -1, True, []), (1, 2, True, []), (-1, 2, True, []))
+    owner_added(0, 0)
+    down.run((2, -1, True, []))
+    down.run((1, 2, True, []))
+    down.run((-1, 2, True, []))
     own_halves([(mate, 2), (-mate, 2)], 0)
     own_halves([(2, 1), (2, -1)], 1)
     owner_added(0, 1)
     half_added(0, 2)
     across_wait(dn, dd, 3)
-    rest_halves([(mate, 2), (-mate, 2)], 0)
+    rest_halves([(mate, 2), (-mate, 2)], 0, False)
+    rest_halves([(2, 1), (2, -1)], 1)
+    near_done([(mate, 2), (-mate, 2)])
     down.run((2, 2, True, []))
-    rest_halves([(2, 1), (2, -1)], 1)
     own_halves([(2, 2)], 0)
     across_wait(dn, dd, 4)
     rest_halves([(2, 2)], 0)

time: 66.9 us -> 65.5 us (0.979)
  the two profiles are of different devices: /device:TPU:33 before, /device:TPU:17 now
where the time goes in v6:
time: 65.5 us; the launch traced here: 65.4 us
  Pallas kernels  64.6 us (99%)
  local copies, waits for them, and re-layouts  0.71 us (1%)
    pallas_call x1, Pallas kernels, body(): pl.pallas_call(kernel, name='layer', out_shape=jax.ShapeDtypeStruct((512,...  64.6 us

profile of v6, /device:TPU:17, one launch (start us, length us, event | category | flops | bytes accessed | tf_op | source)
XLA Modules:
  0.0 65.4 jit_solution(11450177611472619209)
XLA Ops:
  0.0 64.6 %layer.1 = bf16[512,256]{1,0:T(8,128)(2,1)S(1)} custom-call(bf16[512,256]{1,0:T(8,128)(2,1)} %stream.1, f32[1,2048]{1,0:T(1,128)} %bitcast.7, bf16[4,32,64]{2,1,0:T(8,128)(2,1)} %pool_weight.1, f32[1,2048]{1,0:T(1,128)} %bitcast.8, f32[1,2048]{1,0:T(1,128)} %bitcast.9, bf16[704,128]{1,0:T(8,128)(2,1)} %bitcast.5, bf16[704,128]{1,0:T(8,128)(2,1)} %bitcast.6, ...), custom_call_target="tpu_custom_call" | custom-call | tf_op jit(solution)/shard_map/layer/pallas_call | solution.py:567
  64.7 0.7 %copy.12 = bf16[512,256]{1,0:T(8,128)(2,1)} copy(bf16[512,256]{1,0:T(8,128)(2,1)S(1)} %layer.1) | data formatting | bytes 524288

commit v7 on v6

--- a/solution.py
+++ b/solution.py
@@ -27,7 +27,7 @@
     out,
     gu, dn, pw, xs, sv, pv, gv, tv, taps, perm, unperm, band, gains, xg, wg, nf, acc, hid,
     pb, rbuf, sums, relay_in, early,
-    lsem, gsem, dsem, psem, gd, dd, pys, pds, xys, xds, rsem, ssem, relsem,
+    lsem, gsem, dsem, psem, gd, dd, pys, pds, xys, xds, rsem, ssem, relsem, ready,
 ):
     fs, tp = lax.axis_index("fs"), lax.axis_index("tp")
     z, x = fs // 4, fs % 4
@@ -43,7 +43,8 @@
 
     barrier = pltpu.get_barrier_semaphore()
     near = [(dx, dz) for dz in (0, 1, -1) for dx in (0, 1, -1)][1:]
-    peers = [(at_fs(dx, dz), tp) for dx, dz in near]
+    beside = [(at_fs(dx, dz), tp) for dx, dz in near if dx * dz == 0]
+    peers = list(beside)
     peers += [(fs, at_y(dy, core)) for dy in (1, -1) for core in (0, 1)] + [partner]
     for peer in peers:
         pl.semaphore_signal(barrier, inc=1, device_id=peer, device_id_type=MESH)
@@ -149,15 +150,12 @@
         remote(piece(0, p), piece(0, p), ssem.at[3], xys.at[p, 0], (fs, at_y(1, c))).start()
         remote(piece(0, p), piece(0, p), ssem.at[3], xys.at[p, 1], (fs, at_y(-1, c))).start()
 
+    for peer in beside:
+        pl.semaphore_signal(ready, inc=1, device_id=peer, device_id_type=MESH)
     RIGHT, LEFT, UP, DOWN = (1, 0), (-1, 0), (0, 1), (0, -1)
     remote(sv, xs.at[y, c], ssem.at[4], xds.at[0], partner).start()
     piece_out(c)
-    for dx, dz in near:
-        mine = pw.at[tp, fs]
-        remote(mine, mine, ssem.at[0], psem.at[0], (at_fs(dx, dz), tp)).start()
     gup.run((0, 0, False, [RIGHT]))
-    gup.run((0, 0, False, [UP]))
-    gup.run((0, 0, False, [LEFT]))
     across(gu, gd, ssem.at[5])
     for load in loads[5:]:
         load.wait()
@@ -172,6 +170,12 @@
 
     got(xs.at[y, 1 - c], xds.at[0])
     piece_out(1 - c)
+    pl.semaphore_wait(ready, len(beside))
+    for dx, dz in near:
+        mine = pw.at[tp, fs]
+        remote(mine, mine, ssem.at[0], psem.at[0], (at_fs(dx, dz), tp)).start()
+    gup.run((0, 0, False, [UP]))
+    gup.run((0, 0, False, [LEFT]))
 
     three = concat([gv[0], gv[1], gv[2], jnp.zeros((5, 2048), f32)], 0)
     high = three.astype(bf16)
@@ -188,6 +192,7 @@
         taps[core, 0] = tv[0, :, a : a + 704]
         taps[core, 1] = tv[1, :, a : a + 704]
 
+    gup.run((1, 0, True, [RIGHT]))
     got(pw.at[tp, 0:8], psem.at[0])
 
     def onward(ox, oz, half, dx, dz):
@@ -201,13 +206,14 @@
         onward(o, 1, 1, 0, -1)
     onward(-1, -1, 0, 1, 1)
     onward(1, 1, 1, -1, -1)
-    gup.run((1, 0, True, [RIGHT]))
     gup.run((0, 0, False, [DOWN]))
     gup.run((1, 0, False, [UP]))
     got(piece(-1, 0), xys.at[0, 0])
     remote(piece(-1, 0), piece(-1, 0), ssem.at[3], xys.at[0, 2], (fs, at_y(1, c))).start()
     got(piece(1, 1), xys.at[1, 1])
     remote(piece(1, 1), piece(1, 1), ssem.at[3], xys.at[1, 2], (fs, at_y(-1, c))).start()
+    gup.run((2, 0, True, [UP]))
+    gup.run((-1, 0, True, [UP]))
     got(pw.at[tp, 0:7], psem.at[1])
 
     def columns(dy, core):
@@ -228,8 +234,6 @@
     half_out(0, 1, 1, 1)
     half_out(0, 0, 3, -1)
     pool_across(0, 0)
-    gup.run((2, 0, True, [UP]))
-    gup.run((-1, 0, True, [UP]))
     gup.run((0, 1, True, [UP]), (1, 0, False, [DOWN]), (2, 0, False, [DOWN]), (-1, 0, False, [DOWN]))
 
     acc[...] = jnp.zeros_like(acc)
@@ -607,6 +611,7 @@
             DMA((3, 2, 2)),
             DMA((10,)),
             DMA((2, 2, 2)),
+            pltpu.SemaphoreType.REGULAR,
         ],
         compiler_params=pltpu.CompilerParams(
             collective_id=0, has_side_effects=True, vmem_limit_bytes=50 * 1024 * 1024

time: 65.5 us -> 64.9 us (level)
  the two profiles are of different devices: /device:TPU:17 before, /device:TPU:1 now
where the time goes in v7:
time: 64.9 us; the launch traced here: 64.8 us
  Pallas kernels  64.1 us (99%)
  local copies, waits for them, and re-layouts  0.71 us (1%)
    pallas_call x1, Pallas kernels, body(): pl.pallas_call(kernel, name='layer', out_shape=jax.ShapeDtypeStruct((512,...  64.1 us

profile of v7, /device:TPU:1, one launch (start us, length us, event | category | flops | bytes accessed | tf_op | source)
XLA Modules:
  0.0 64.8 jit_solution(8401809914476963436)
XLA Ops:
  0.0 64.1 %layer.1 = bf16[512,256]{1,0:T(8,128)(2,1)S(1)} custom-call(bf16[512,256]{1,0:T(8,128)(2,1)} %stream.1, f32[1,2048]{1,0:T(1,128)} %bitcast.7, bf16[4,32,64]{2,1,0:T(8,128)(2,1)} %pool_weight.1, f32[1,2048]{1,0:T(1,128)} %bitcast.8, f32[1,2048]{1,0:T(1,128)} %bitcast.9, bf16[704,128]{1,0:T(8,128)(2,1)} %bitcast.5, bf16[704,128]{1,0:T(8,128)(2,1)} %bitcast.6, ...), custom_call_target="tpu_custom_call" | custom-call | tf_op jit(solution)/shard_map/layer/pallas_call | solution.py:571
  64.1 0.7 %copy.12 = bf16[512,256]{1,0:T(8,128)(2,1)} copy(bf16[512,256]{1,0:T(8,128)(2,1)S(1)} %layer.1) | data formatting | bytes 524288
